TPU v7x, 512 devices: a whole 4x8x8 slice. The times are simulated.
512 devices in a mesh: dp: 4 (over x), kv: 64 (over z, y), tp: 2 (over core).
Axes of the slice: x: 4, y: 8, z: 8, core: 2. Of those that a mesh axis runs over, the one named last changes fastest.
Arguments:
- tokens: bfloat16 [32, 1024], P('dp', 'kv'), may hold values from -6 to 6
- norm_gain: float32 [1024], P('kv'), may hold values from 0.1 to 1.9
- w_query: bfloat16 [1024, 4, 64], P('kv', 'tp'), may hold values from -0.1875 to 0.1875
- w_key: bfloat16 [1024, 4, 64], P('kv', 'tp'), may hold values from -0.1875 to 0.1875
- w_value: bfloat16 [1024, 4, 64], P('kv', 'tp'), may hold values from -0.1875 to 0.1875
- w_gate: bfloat16 [1024, 4, 64], P('kv', 'tp'), may hold values from -0.1875 to 0.1875
- w_forget: bfloat16 [1024, 4], P('kv', 'tp'), may hold values from -0.1875 to 0.1875
- w_out: bfloat16 [4, 64, 1024], P('tp', None, 'kv'), may hold values from -0.375 to 0.375
- cache_key: bfloat16 [32, 32768, 4, 64], P('dp', 'kv', 'tp'), may hold values from -6 to 6
- cache_value: bfloat16 [32, 32768, 4, 64], P('dp', 'kv', 'tp'), may hold values from -6 to 6
- cache_logf: float32 [32, 32768, 4], P('dp', 'kv', 'tp'), may hold values from -0.60003052 to 0, as said below
- lengths: int32 [32], P('dp'), may hold values from 31744 to 32767
Outputs:
- mixed: float32 [32, 1024], P('dp', 'kv')
- new_key: bfloat16 [32, 4, 64], P('dp', 'tp')
- new_value: float32 [32, 4, 64], P('dp', 'tp')
- new_logf: float32 [32, 4], P('dp', 'tp')
Inputs may be any that keep to these rules, and one draw needn't show every extreme that they name: `lengths`: each sequence has between 31744 and 32767 cached tokens. `cache_logf`: log forget gates are at most 0; most are small (down to -1 / 32768, with a typical size that differs by head), and about six positions of each sequence and head hold drops of 0.2 to 0.6.
All inputs are finite; a program needn't handle non-finite values.
Results may differ from a plain program's by a relative error of at most 0.0095.
Values sent between devices are 32-bit elements.
No kernel may reach another device: no remote copies, remote signals or barrier semaphores. Data moves between devices by JAX's collectives and lax.ppermute only.
A program may use at most 64 MiB of HBM per device.

v0:
```python
import jax
import jax.numpy as jnp
from jax import lax
from jax.sharding import Mesh
from jax.sharding import PartitionSpec as P

D = 1024
HEAD_DIM = 64
KV = ("kv_0", "kv_1")


eps = 1e-06
very_low = -1e30


def by_axis(value, axes):
    for axis in axes:
        value = lax.psum(value, axis)
    return value


def neutral_like(value, identity):
    return jax.tree.map(
        lambda part, zero: jnp.zeros_like(part) + jnp.asarray(zero, part.dtype), value, identity
    )


def prefix_by_axis(value, axes, combine, identity, reverse):
    before = start = neutral_like(value, identity)
    so_far = value
    for axis in reversed(axes):
        devices, here = lax.axis_size(axis), lax.axis_index(axis)
        pieces = jax.tree.map(lambda part: lax.all_gather(part, axis), so_far)
        inside, so_far = start, start
        for k in reversed(range(devices)) if reverse else range(devices):
            passed = k > here if reverse else k < here
            so_far = combine(so_far, jax.tree.map(lambda part: part[k], pieces))
            inside = jax.tree.map(lambda new, old: jnp.where(passed, new, old), so_far, inside)
        before = combine(inside, before)
    return before


def one_axis_at_a_time(value, axes):
    for axis in axes:
        value = lax.pmax(value, axis)
    return value


def total_of_pieces(value, axis):
    return lax.all_gather(value, axis).sum(0)


def add_terms(earlier, later):
    return earlier + later


def head_norm(values):
    return values * lax.rsqrt(jnp.mean(values * values, axis=-1, keepdims=True) + eps)


def on_device(
    tokens,
    norm_gain,
    w_query,
    w_key,
    w_value,
    w_gate,
    w_forget,
    w_out,
    cache_key,
    cache_value,
    cache_logf,
    lengths,
):
    wide_tokens = tokens.astype(jnp.float32)
    local_squares = jnp.sum(wide_tokens * wide_tokens, axis=1)
    total_squares = by_axis(local_squares, KV)
    inv_root = lax.rsqrt(total_squares / D + eps)
    normed = (wide_tokens * inv_root[:, None] * norm_gain).astype(jnp.bfloat16)
    part_query = jnp.einsum("sd,dhe->she", normed, w_query, preferred_element_type=jnp.float32)
    part_key = jnp.einsum("sd,dhe->she", normed, w_key, preferred_element_type=jnp.float32)
    part_value = jnp.einsum("sd,dhe->she", normed, w_value, preferred_element_type=jnp.float32)
    part_gate = jnp.einsum("sd,dhe->she", normed, w_gate, preferred_element_type=jnp.float32)
    part_forget = jnp.dot(normed, w_forget, preferred_element_type=jnp.float32)
    proj_query, proj_key, proj_value, proj_gate, proj_forget = (
        by_axis(part_query, KV),
        by_axis(part_key, KV),
        by_axis(part_value, KV),
        by_axis(part_gate, KV),
        by_axis(part_forget, KV),
    )
    query_vec = head_norm(proj_query).astype(jnp.bfloat16)
    key_new = head_norm(proj_key).astype(jnp.bfloat16)
    value_new = proj_value
    gate_silu = jax.nn.silu(proj_gate)
    logf_new = jax.nn.log_sigmoid(proj_forget)
    span = cache_key.shape[1]
    shard_index = lax.axis_index(KV)
    positions = shard_index * span + jnp.arange(span, dtype=jnp.int32)
    in_range = positions[None, :] < lengths[:, None]
    masked_logf = jnp.where(in_range[:, :, None], cache_logf, jnp.float32(0.0))
    running = jnp.cumsum(masked_logf, axis=1)
    shard_total = running[:, -1, :]
    later_outside = prefix_by_axis(shard_total, KV, add_terms, jnp.zeros_like(shard_total), True)
    forget_bias = (
        logf_new[:, None, :] + (shard_total[:, None, :] - running) + later_outside[:, None, :]
    )
    scores = jnp.einsum(
        "she,sphe->shp", query_vec, cache_key, preferred_element_type=jnp.float32
    ) * HEAD_DIM ** (-0.5)
    scores = scores + jnp.transpose(forget_bias, (0, 2, 1))
    score_new = jnp.sum(
        query_vec.astype(jnp.float32) * key_new.astype(jnp.float32), axis=-1
    ) * HEAD_DIM ** (-0.5)
    holder = lengths // span == shard_index
    range_mask = in_range[:, None, :]
    local_peak = jnp.max(jnp.where(range_mask, scores, very_low), axis=-1)
    local_peak = jnp.maximum(local_peak, jnp.where(holder[:, None], score_new, very_low))

    def partial_terms(peak):
        weights = jnp.where(range_mask, jnp.exp(scores - peak[..., None]), jnp.float32(0.0))
        weight_new = jnp.where(holder[:, None], jnp.exp(score_new - peak), jnp.float32(0.0))
        denominator = jnp.sum(weights, axis=-1) + weight_new
        weighted = jnp.einsum(
            "shp,sphe->she",
            weights.astype(jnp.bfloat16),
            cache_value,
            preferred_element_type=jnp.float32,
        )
        weighted = weighted + weight_new[..., None] * value_new
        return (denominator, weighted)

    peak = one_axis_at_a_time(local_peak, KV)
    local_den, local_sum = partial_terms(peak)
    denominator, weighted = (by_axis(local_den, KV), by_axis(local_sum, KV))
    attended = weighted / denominator[..., None]
    gated = (head_norm(attended) * gate_silu).astype(jnp.bfloat16)
    partial_out = jnp.einsum("she,hed->sd", gated, w_out, preferred_element_type=jnp.float32)
    mixed = total_of_pieces(partial_out, "tp")
    return (mixed, key_new, value_new, logf_new)


def solution(mesh):
    finer = Mesh(
        mesh.devices.reshape(mesh.shape["dp"], 8, 8, mesh.shape["tp"]), ("dp", "kv_0", "kv_1", "tp")
    )
    return jax.shard_map(
        on_device,
        mesh=finer,
        in_specs=(
            P("dp", KV),
            P(KV),
            P(KV, "tp", None),
            P(KV, "tp", None),
            P(KV, "tp", None),
            P(KV, "tp", None),
            P(KV, "tp"),
            P("tp", None, KV),
            P("dp", KV, "tp", None),
            P("dp", KV, "tp", None),
            P("dp", KV, "tp"),
            P("dp"),
        ),
        out_specs=(P("dp", KV), P("dp", "tp", None), P("dp", "tp", None), P("dp", "tp")),
        check_vma=False,
    )
```

profile of v0, /device:TPU:1, one launch (start us, length us, event | category | flops | bytes accessed | tf_op | source)
XLA Modules:
  0.0 236.8 jit_solution(5692271520904168080)
XLA Ops:
  0.6 0.0 copy-start
  0.6 0.0 copy-start.2
  0.7 0.9 fusion.19
  1.5 20.2 %psum.112 = f32[8]{0:T(128)S(1)} all-reduce(f32[8]{0:T(128)S(1)} %fusion.19), channel_id=1, replica_groups=mesh['dp'=4,'kv_0'=8,'kv_1'=8,'tp'=2] {'kv_0'}, use_global_device_ids=true, to_apply=%region_1.0 | all-reduce | flops 8 | bytes 64 | tf_op jit(solution)/shard_map/psum | solution.py:18
  21.8 13.8 %psum.113 = f32[8]{0:T(128)S(1)} all-reduce(f32[8]{0:T(128)S(1)} %psum.112), channel_id=1, replica_groups=mesh['dp'=4,'kv_0'=8,'kv_1'=8,'tp'=2] {'kv_1'}, use_global_device_ids=true, to_apply=%region_2.0 | all-reduce | flops 8 | bytes 64 | tf_op jit(solution)/shard_map/psum | solution.py:18
  35.6 0.8 fusion.21
  36.4 0.0 copy-done.2
  36.4 0.1 fusion.11
  36.5 0.7 copy-done.7
  37.2 0.1 broadcast_compare_fusion
  37.4 2.3 reduce-window.6
  39.6 0.1 slice.84
  39.7 0.1 copy.48
  39.9 0.1 bitcast_bitcast_fusion
  39.9 0.2 slice_reduce_fusion
  40.1 18.1 %all-gather = f32[64,1,2]{1,0,2:T(8,128)S(1)} all-gather(f32[8,1,2]{1,0,2:T(8,128)S(1)} %get-tuple-element.45), channel_id=2, replica_groups=mesh['dp'=4,'kv_0'=8,'kv_1'=8,'tp'=2] {'kv_1'}, dimensions={0}, use_global_device_ids=true | all-gather | bytes 576 | tf_op jit(solution)/shard_map/all_gather | solution.py:33
  58.2 0.1 select_reduce_fusion.1
  58.3 10.1 %all_gather.14 = f32[8,8,2]{1,2,0:T(2,128)S(1)} all-gather(f32[1,8,2]{1,2,0:T(2,128)S(1)} %bitcast.57), channel_id=1, replica_groups=mesh['dp'=4,'kv_0'=8,'kv_1'=8,'tp'=2] {'kv_0'}, dimensions={0}, use_global_device_ids=true | all-gather | bytes 576 | tf_op jit(solution)/shard_map/all_gather | solution.py:33
  68.4 0.7 copy-done.3
  69.1 0.1 fusion.17
  69.2 0.5 copy-done.10
  69.8 0.1 fusion.37
  69.9 0.1 fusion.15
  70.0 0.6 copy-done.5
  70.6 0.1 fusion.13
  70.7 21.2 %all-reduce.3 = (f32[8,2,64]{2,0,1:T(8,128)S(1)}, f32[8,2]{0,1:T(2,128)S(1)}, f32[8,2,64]{2,0,1:T(8,128)S(1)}, f32[8,2,64]{2,0,1:T(8,128)S(1)}) all-reduce(f32[8,2,64]{2,0,1:T(8,128)S(1)} %fusion.17, f32[8,2]{0,1:T(2,128)S(1)} %fusion.37, f32[8,2,64]{2,0,1:T(8,128)S(1)} %fusion.15, ...), channel_id=1, replica_groups=mesh['dp'=4,'kv_0'=8,'kv_1'=8,'tp'=2] {'kv_0'}, use_global_device_ids=true, to_apply=%region_3.0 | all-reduce | flops 3088 | bytes 24704 | tf_op jit(solution)/shard_map/psum | solution.py:18
  91.9 20.8 %all-reduce.1 = (f32[8,2,64]{2,0,1:T(8,128)S(1)}, f32[8,2]{0,1:T(2,128)S(1)}, f32[8,2,64]{2,0,1:T(8,128)S(1)}, f32[8,2,64]{2,0,1:T(8,128)S(1)}) all-reduce(f32[8,2,64]{2,0,1:T(8,128)S(1)} %get-tuple-element.32, f32[8,2]{0,1:T(2,128)S(1)} %get-tuple-element.33, ...), channel_id=1, replica_groups=mesh['dp'=4,'kv_0'=8,'kv_1'=8,'tp'=2] {'kv_1'}, use_global_device_ids=true, to_apply=%region_4.0 | all-reduce | flops 3088 | bytes 24704 | tf_op jit(solution)/shard_map/psum | solution.py:18
  112.8 0.0 copy-start.6
  112.8 0.1 multiply_reduce_fusion.2
  112.9 0.2 multiply_reduce_fusion.1
  113.0 0.0 copy-done
  113.0 0.3 fusion.9
  113.3 0.0 copy-done.6
  113.3 0.2 select_reduce_fusion
  113.5 10.7 %pmax.14 = f32[8,2]{0,1:T(2,128)S(1)} all-reduce(f32[8,2]{0,1:T(2,128)S(1)} %select_maximum_fusion), channel_id=1, replica_groups=mesh['dp'=4,'kv_0'=8,'kv_1'=8,'tp'=2] {'kv_0'}, use_global_device_ids=true, to_apply=%region_15.16 | all-reduce | flops 16 | bytes 128 | tf_op jit(solution)/shard_map/pmax | solution.py:45
  124.2 10.7 %pmax.15 = f32[8,2]{0,1:T(2,128)S(1)} all-reduce(f32[8,2]{0,1:T(2,128)S(1)} %pmax.14), channel_id=1, replica_groups=mesh['dp'=4,'kv_0'=8,'kv_1'=8,'tp'=2] {'kv_1'}, use_global_device_ids=true, to_apply=%region_16.17 | all-reduce | flops 16 | bytes 128 | tf_op jit(solution)/shard_map/pmax | solution.py:45
  134.9 0.2 fusion.5
  135.0 0.4 fusion.3
  135.4 0.1 bitcast_add_fusion
  135.5 22.0 %all-reduce.2 = (f32[8,2,64]{2,0,1:T(8,128)S(1)}, f32[8,2,64]{2,0,1:T(8,128)S(1)}, f32[8,2]{0,1:T(2,128)S(1)}) all-reduce(f32[8,2,64]{2,0,1:T(8,128)S(1)} %fusion.11, f32[8,2,64]{2,0,1:T(8,128)S(1)} %bitcast_add_fusion, f32[8,2]{0,1:T(2,128)S(1)} %get-tuple-element.36), channel_id=1, replica_groups=mesh['dp'=4,'kv_0'=8,'kv_1'=8,'tp'=2] {'kv_0'}, use_global_device_ids=true, to_apply=%region_25.26 | all-reduce | flops 2064 | bytes 16512 | tf_op jit(solution)/shard_map/psum | solution.py:18
  157.5 21.8 %all-reduce = (f32[8,2,64]{2,0,1:T(8,128)S(1)}, f32[8,2,64]{2,0,1:T(8,128)S(1)}, f32[8,2]{0,1:T(2,128)S(1)}) all-reduce(f32[8,2,64]{2,0,1:T(8,128)S(1)} %get-tuple-element.29, f32[8,2,64]{2,0,1:T(8,128)S(1)} %get-tuple-element.30, f32[8,2]{0,1:T(2,128)S(1)} %get-tuple-element.31), channel_id=1, replica_groups=mesh['dp'=4,'kv_0'=8,'kv_1'=8,'tp'=2] {'kv_1'}, use_global_device_ids=true, to_apply=%region_26.27 | all-reduce | flops 2064 | bytes 16512 | tf_op jit(solution)/shard_map/psum | solution.py:18
  179.3 0.2 multiply_reduce_fusion
  179.5 0.5 copy-done.9
  180.0 0.2 convolution_bitcast_fusion
  180.2 54.9 %all-gather.1 = f32[16,16]{1,0:T(8,128)S(1)} all-gather(f32[8,16]{1,0:T(8,128)S(1)} %convolution_bitcast_fusion), channel_id=3, replica_groups=mesh['dp'=4,'kv_0'=8,'kv_1'=8,'tp'=2] {'tp'}, dimensions={0}, use_global_device_ids=true | all-gather | bytes 1536 | tf_op jit(solution)/shard_map/all_gather | solution.py:50
  235.0 0.6 bitcast_reduce_fusion
  235.6 0.6 copy.54
  236.2 0.6 copy.55
  (27 shorter events, 0.2 us)
Async XLA Ops:
  0.6 112.4 %copy-start = (bf16[8,512,2,64]{1,3,2,0:T(8,128)(2,1)S(1)}, bf16[8,512,2,64]{1,3,2,0:T(8,128)(2,1)}, u32[]{:S(2)}) copy-start(bf16[8,512,2,64]{1,3,2,0:T(8,128)(2,1)} %param.20) | copy-start | bytes 3145732
  0.6 35.8 %copy-start.2 = (bf16[16,2,64]{2,1,0:T(2,128)(2,1)S(1)}, bf16[16,2,64]{2,1,0:T(2,128)(2,1)}, u32[]{:S(2)}) copy-start(bf16[16,2,64]{2,1,0:T(2,128)(2,1)} %param.17) | copy-start | bytes 12292
  0.7 36.6 %copy-start.1 = (f32[8,512,2]{1,2,0:T(2,128)S(1)}, f32[8,512,2]{1,2,0:T(2,128)}, u32[]{:S(2)}) copy-start(f32[8,512,2]{1,2,0:T(2,128)} %param.22) | copy-start | bytes 98308
  36.5 0.7 copy-start.7
  68.4 0.7 copy-start.3
  69.1 0.7 copy-start.10
  69.1 0.8 copy-start.4
  69.9 0.7 copy-start.5
  69.9 65.1 %copy-start.8 = (bf16[8,512,2,64]{1,3,2,0:T(8,128)(2,1)S(1)}, bf16[8,512,2,64]{1,3,2,0:T(8,128)(2,1)}, u32[]{:S(2)}) copy-start(bf16[8,512,2,64]{1,3,2,0:T(8,128)(2,1)} %param.21) | copy-start | bytes 3145732
  112.8 0.6 copy-start.6
  179.3 0.7 copy-start.9
where the time goes:
time: 237 us
  blocking collectives  224 us (95%)
  other arithmetic  5.72 us (2%)
  local copies, waits for them, and re-layouts  4.66 us (2%)
    psum x6, blocking collectives, by_axis(): value = lax.psum(value, axis)  120 us
    all_gather x1, blocking collectives, total_of_pieces(): return lax.all_gather(value, axis).sum(0)  54.9 us
    all_gather x2, blocking collectives, prefix_by_axis(): pieces = jax.tree.map(lambda part: lax.all_gather(part, axis), so_far)  28.2 us
    pmax x2, blocking collectives, one_axis_at_a_time(): value = lax.pmax(value, axis)  21.3 us

commit v1 on v0

v1 whole, which is shorter than its diff:
```python
import jax
import jax.numpy as jnp
from jax import lax
from jax.sharding import Mesh
from jax.sharding import PartitionSpec as P

D = 1024
HEAD_DIM = 64
KV = ("kv_0", "kv_1")
N_KV = 64

eps = 1e-06
very_low = -1e30
HI = lax.Precision.HIGHEST


def head_norm(values):
    return values * lax.rsqrt(jnp.mean(values * values, axis=-1, keepdims=True) + eps)


def exchange(slots):
    return lax.all_to_all(slots, KV, 0, 0, tiled=True)


def on_device(
    tokens,
    norm_gain,
    w_query,
    w_key,
    w_value,
    w_gate,
    w_forget,
    w_out,
    cache_key,
    cache_value,
    cache_logf,
    lengths,
):
    seqs, heads = tokens.shape[0], w_query.shape[1]
    wide_tokens = tokens.astype(jnp.float32)
    local_squares = jnp.sum(wide_tokens * wide_tokens, axis=1)
    scaled = wide_tokens * norm_gain

    def project(weight):
        return jnp.dot(
            scaled, weight.reshape(weight.shape[0], -1).astype(jnp.float32), precision=HI
        )

    part_query, part_key, part_value, part_gate = map(project, (w_query, w_key, w_value, w_gate))
    part_forget = project(w_forget)

    span = cache_key.shape[1]
    shard_index = lax.axis_index(KV)
    positions = shard_index * span + jnp.arange(span, dtype=jnp.int32)
    in_range = positions[None, :] < lengths[:, None]
    masked_logf = jnp.where(in_range[:, :, None], cache_logf, jnp.float32(0.0))
    shard_total = jnp.sum(masked_logf, axis=1)

    def spread(row):
        return jnp.broadcast_to(row.reshape(1, -1), (N_KV, row.size))

    pieces = [p.reshape(N_KV, -1) for p in (part_key, part_value, part_gate)]
    tail = [spread(local_squares), spread(part_forget), spread(shard_total)] + pieces
    tail = jnp.concatenate(tail, axis=1)
    tail = jnp.pad(tail, ((0, 0), (0, 128 - tail.shape[1])))
    first = jnp.concatenate(
        [jnp.broadcast_to(part_query[None], (N_KV, seqs, 128)), tail[:, None, :]], axis=1
    )
    first = exchange(first)
    summed = jnp.sum(first, axis=0)
    raw_query = summed[:seqs].reshape(seqs, heads, HEAD_DIM)
    sums = summed[seqs]
    inv_root = lax.rsqrt(sums[:seqs] / D + eps)
    forget = sums[seqs : seqs + 16].reshape(seqs, heads) * inv_root[:, None]
    logf_new = jax.nn.log_sigmoid(forget)
    totals = first[:, seqs, 24:40].reshape(N_KV, seqs, heads)
    own_pieces = sums[40:88]
    query_vec = head_norm(raw_query * inv_root[:, None, None]).astype(jnp.bfloat16)

    upper = (
        jnp.arange(span, dtype=jnp.int32)[:, None] > jnp.arange(span, dtype=jnp.int32)[None, :]
    ).astype(jnp.float32)
    later_inside = jnp.einsum("sph,pt->sht", masked_logf, upper, precision=HI)
    scores = jnp.einsum(
        "she,sphe->shp", query_vec, cache_key, preferred_element_type=jnp.float32
    ) * HEAD_DIM ** (-0.5)
    scores = scores + later_inside
    range_mask = in_range[:, None, :]
    local_peak = jnp.max(jnp.where(range_mask, scores, very_low), axis=-1)
    weights = jnp.where(range_mask, jnp.exp(scores - local_peak[..., None]), jnp.float32(0.0))
    local_den = jnp.sum(weights, axis=-1)
    local_sum = jnp.einsum(
        "shp,sphe->she",
        weights.astype(jnp.bfloat16),
        cache_value,
        preferred_element_type=jnp.float32,
    )

    row = jnp.concatenate([local_den.reshape(-1), local_peak.reshape(-1), own_pieces])
    row = jnp.pad(row, (0, 128 - row.shape[0]))
    second = jnp.concatenate([local_sum.reshape(seqs, 128), row[None]], axis=0)
    second = exchange(jnp.broadcast_to(second[None], (N_KV, seqs + 1, 128)))

    later = (
        jnp.arange(N_KV, dtype=jnp.int32)[None, :] > jnp.arange(N_KV, dtype=jnp.int32)[:, None]
    ).astype(jnp.float32)
    later_outside = jnp.einsum("ij,jsh->ish", later, totals, precision=HI)

    back = second[:, seqs]
    whole_key, whole_value, whole_gate = (
        back[:, 32 + 16 * n : 48 + 16 * n].reshape(seqs, heads, HEAD_DIM)
        * inv_root[:, None, None]
        for n in range(3)
    )
    key_new = head_norm(whole_key).astype(jnp.bfloat16)
    value_new = whole_value
    gate_silu = jax.nn.silu(whole_gate)
    score_new = jnp.sum(
        query_vec.astype(jnp.float32) * key_new.astype(jnp.float32), axis=-1
    ) * HEAD_DIM ** (-0.5)
    dens = back[:, :16].reshape(N_KV, seqs, heads)
    peaks = back[:, 16:32].reshape(N_KV, seqs, heads) + later_outside + logf_new[None]
    peak = jnp.maximum(jnp.max(peaks, axis=0), score_new)
    factors = jnp.exp(peaks - peak[None])
    weight_new = jnp.exp(score_new - peak)
    denominator = jnp.sum(factors * dens, axis=0) + weight_new
    parts = second[:, :seqs].reshape(N_KV, seqs, heads, HEAD_DIM)
    weighted = jnp.sum(factors[..., None] * parts, axis=0) + weight_new[..., None] * value_new
    attended = weighted / denominator[..., None]
    gated = (head_norm(attended) * gate_silu).astype(jnp.bfloat16)
    partial_out = jnp.einsum("she,hed->sd", gated, w_out, preferred_element_type=jnp.float32)
    mixed = lax.all_gather(partial_out, "tp").sum(0)
    return (mixed, key_new, value_new, logf_new)


def solution(mesh):
    finer = Mesh(
        mesh.devices.reshape(mesh.shape["dp"], 8, 8, mesh.shape["tp"]), ("dp", "kv_0", "kv_1", "tp")
    )
    return jax.shard_map(
        on_device,
        mesh=finer,
        in_specs=(
            P("dp", KV),
            P(KV),
            P(KV, "tp", None),
            P(KV, "tp", None),
            P(KV, "tp", None),
            P(KV, "tp", None),
            P(KV, "tp"),
            P("tp", None, KV),
            P("dp", KV, "tp", None),
            P("dp", KV, "tp", None),
            P("dp", KV, "tp"),
            P("dp"),
        ),
        out_specs=(P("dp", KV), P("dp", "tp", None), P("dp", "tp", None), P("dp", "tp")),
        check_vma=False,
    )
```

time: 237 us -> 79.4 us (0.34)
  blocking collectives: 224 us -> 40.2 us
  waiting for transfers between devices: 0 us -> 16.3 us
  starting transfers between devices: 0 us -> 6.62 us
  local copies, waits for them, and re-layouts: 4.66 us -> 9.44 us
    psum x6 -> x0, blocking collectives: 120 us -> none  [by_axis(): value = lax.psum(value, axis)]
    all_gather x3 -> x1, blocking collectives: 83.1 us -> 5.26 us  [on_device(): mixed = lax.all_gather(partial_out, 'tp').sum(0)]
    all_to_all x0 -> x1, blocking collectives: none -> 34.9 us  [exchange(): return lax.all_to_all(slots, KV, 0, 0, tiled=True)]
    pmax x2 -> x0, blocking collectives: 21.3 us -> none  [one_axis_at_a_time(): value = lax.pmax(value, axis)]
    all_to_all x0 -> x1, waiting for transfers between devices: none -> 16.3 us  [exchange(): return lax.all_to_all(slots, KV, 0, 0, tiled=True)]
    all_to_all x0 -> x1, starting transfers between devices: none -> 6.62 us  [exchange(): return lax.all_to_all(slots, KV, 0, 0, tiled=True)]
    another operation x3 -> x0, other arithmetic: 2.39 us -> none
    unnamed x24 -> x28, local copies, waits for them, and re-layouts: 4.25 us -> 4.84 us
  transfers between devices with their start and end apart: 0 -> 1, of which waited for: 0 -> 1; matrix products, arithmetic and copies ran while one was open for 0% -> 1% of each run, Pallas kernels for 0% -> 0%
where the time goes in v1:
time: 79.4 us; the launch traced here: 78.8 us
  blocking collectives  40.2 us (51%)
  waiting for transfers between devices  16.3 us (21%)
  local copies, waits for them, and re-layouts  9.44 us (12%)
  starting transfers between devices  6.62 us (8%)
  other arithmetic  3.59 us (5%)
  matrix products  1.89 us (2%)
  between operations  0.87 us (1%)
    all_to_all x1, blocking collectives, exchange(): return lax.all_to_all(slots, KV, 0, 0, tiled=True)  34.9 us
    all_to_all x1, waiting for transfers between devices, exchange(): return lax.all_to_all(slots, KV, 0, 0, tiled=True)  16.3 us
    all_to_all x1, starting transfers between devices, exchange(): return lax.all_to_all(slots, KV, 0, 0, tiled=True)  6.62 us
    all_gather x1, blocking collectives, on_device(): mixed = lax.all_gather(partial_out, 'tp').sum(0)  5.26 us
    unnamed x28, local copies, waits for them, and re-layouts  4.84 us
  transfers between devices with their start and end apart: 1, of which 1 were waited for; matrix products, arithmetic and copies ran while one was open for 1% of the time, Pallas kernels for 0%

profile of v1, /device:TPU:1, one launch (start us, length us, event | category | flops | bytes accessed | tf_op | source)
XLA Modules:
  0.0 78.8 jit_solution(16611075115997351626)
XLA Ops:
  0.7 0.7 copy-done.1
  1.4 0.1 fusion.23
  1.6 0.1 reshape.221
  1.7 0.6 copy-done.5
  2.2 0.1 reshape.222
  2.3 0.6 copy-done.3
  2.9 0.1 fusion.22
  3.0 0.1 fusion.20
  3.1 0.5 copy-done.6
  3.6 0.1 reshape.224
  3.7 0.1 fusion.19
  3.8 0.6 copy-done.7
  4.4 0.1 reshape.226
  4.5 0.1 fusion.18
  4.6 0.5 copy-done.10
  5.1 0.1 fusion.21
  5.6 0.6 copy-done.11
  6.2 0.1 fusion.36
  6.4 0.1 concatenate.12
  6.6 34.9 %all_to_all.10 = f32[64,9,128]{2,1,0:T(8,128)S(1)} all-to-all(f32[64,9,128]{2,1,0:T(8,128)S(1)} %pad_maximum_fusion), channel_id=1, replica_groups=mesh['dp'=4,'kv_0'=8,'kv_1'=8,'tp'=2] {'kv_0','kv_1'}, dimensions={0} | all-to-all | bytes 589824 | tf_op jit(solution)/shard_map/all_to_all | solution.py:22
  41.8 0.2 multiply_reduce_fusion.3
  42.0 0.1 fusion.47
  42.1 0.2 fusion.13
  42.3 0.4 select_reduce_fusion
  42.8 0.2 fusion.11
  43.0 0.4 fusion.4
  43.7 0.1 fusion.31
  43.8 0.8 %broadcast_in_dim.65 = f32[64,9,128]{2,1,0:T(8,128)} broadcast(f32[9,128]{1,0:T(8,128)S(1)} %pad_maximum_fusion.1), dimensions={1,2} | broadcast | bytes 299520 | tf_op jit(solution)/shard_map/broadcast_in_dim | solution.py:102
  44.6 6.6 %all-to-all-start.1 = ((f32[64,9,128]{2,1,0:T(8,128)}), f32[64,9,128]{2,1,0:T(8,128)S(1)}, u32[]{:S(2)}, u32[]{:S(2)}) async-start(f32[64,9,128]{2,1,0:T(8,128)} %broadcast_in_dim.65), calls=%async_computation.1 | async-start | bytes 1048576 | tf_op jit(solution)/shard_map/all_to_all | solution.py:22
  51.2 0.1 slice.63
  51.4 0.1 slice_reduce_fusion
  51.6 0.1 fusion.24
  51.7 0.1 copy.69
  51.8 16.3 %all-to-all-done.1 = f32[64,9,128]{2,1,0:T(8,128)S(1)} async-done(((f32[64,9,128]{2,1,0:T(8,128)}), f32[64,9,128]{2,1,0:T(8,128)S(1)}, u32[]{:S(2)}, u32[]{:S(2)}) %all-to-all-start.1) | async-done | bytes 294944 | tf_op jit(solution)/shard_map/all_to_all | solution.py:22
  68.1 0.1 copy.85
  68.7 0.2 multiply_reduce_fusion.2
  68.8 0.7 multiply_reduce_fusion.1
  69.6 0.2 fusion.38
  69.8 0.2 fusion.15
  70.2 0.2 copy.72
  70.4 0.6 mul.160
  71.0 0.3 mul.161
  71.5 0.7 multiply_reduce_fusion
  72.2 0.1 fusion.17
  72.3 0.6 copy-done.8
  72.9 0.1 convolution_bitcast_fusion
  73.0 5.3 %all-gather = f32[16,16]{1,0:T(8,128)S(1)} all-gather(f32[8,16]{1,0:T(8,128)S(1)} %convolution_bitcast_fusion), channel_id=2, replica_groups=mesh['dp'=4,'kv_0'=8,'kv_1'=8,'tp'=2] {'tp'}, dimensions={0}, use_global_device_ids=true | all-gather | bytes 1536 | tf_op jit(solution)/shard_map/all_gather | solution.py:132
  78.2 0.6 bitcast_reduce_fusion
  (62 shorter events, 2.4 us)
Async XLA Ops:
  0.6 41.4 %copy-start = (bf16[8,512,2,64]{1,3,2,0:T(8,128)(2,1)S(1)}, bf16[8,512,2,64]{1,3,2,0:T(8,128)(2,1)}, u32[]{:S(2)}) copy-start(bf16[8,512,2,64]{1,3,2,0:T(8,128)(2,1)} %param.20) | copy-start | bytes 3145732
  0.7 0.8 copy-start.1
  0.7 0.9 %copy-start.4 = (bf16[16,2,64]{2,1,0:T(2,128)(2,1)S(1)}, bf16[16,2,64]{2,1,0:T(2,128)(2,1)}, u32[]{:S(2)}) copy-start(bf16[16,2,64]{2,1,0:T(2,128)(2,1)} %param.14) | copy-start | bytes 12292
  1.5 0.7 copy-start.5
  2.2 0.7 copy-start.3
  2.9 0.7 copy-start.6
  3.7 0.7 copy-start.7
  4.5 0.7 copy-start.10
  5.4 0.8 %copy-start.2 = (f32[8,512,2]{1,2,0:T(2,128)S(1)}, f32[8,512,2]{1,2,0:T(2,128)}, u32[]{:S(2)}) copy-start(f32[8,512,2]{1,2,0:T(2,128)} %param.22) | copy-start | bytes 98308
  5.5 0.7 copy-start.11
  41.5 1.4 %copy-start.12 = (bf16[8,512,2,64]{1,3,2,0:T(8,128)(2,1)S(1)}, bf16[8,512,2,64]{1,3,2,0:T(8,128)(2,1)}, u32[]{:S(2)}) copy-start(bf16[8,512,2,64]{1,3,2,0:T(8,128)(2,1)} %param.21) | copy-start | bytes 3145732
  44.6 23.4 %all-to-all-start.1 = ((f32[64,9,128]{2,1,0:T(8,128)}), f32[64,9,128]{2,1,0:T(8,128)S(1)}, u32[]{:S(2)}, u32[]{:S(2)}) async-start(f32[64,9,128]{2,1,0:T(8,128)} %broadcast_in_dim.65), calls=%async_computation.1 | async-start | bytes 1048576 | tf_op jit(solution)/shard_map/all_to_all | solution.py:22
  51.8 17.9 %copy-start.9 = (f32[8,2]{0,1:T(2,128)}, f32[8,2]{0,1:T(2,128)S(1)}, u32[]{:S(2)}) copy-start(f32[8,2]{0,1:T(2,128)S(1)} %copy.69) | copy-start | bytes 196
  72.2 0.7 copy-start.8

commit v2 on v1

v2 whole, which is shorter than its diff:
```python
import jax
import jax.numpy as jnp
from jax import lax
from jax.experimental import pallas as pl
from jax.experimental.pallas import tpu as pltpu
from jax.sharding import Mesh
from jax.sharding import PartitionSpec as P

D = 1024
HEAD_DIM = 64
KV = ("kv_0", "kv_1")
N_KV = 64
SEQS = 8
ROWS = 9
VMEM = 16 * 2**20
SPAN = 512
LANES = 128

eps = 1e-06
very_low = -1e30
HI = lax.Precision.HIGHEST
F32 = jnp.float32
NT = (((1,), (1,)), ((), ()))

FORGET, TOTAL, PIECES, PIECE = 8, 24, 40, 16


def iota(shape, dim):
    return lax.broadcasted_iota(jnp.int32, shape, dim)


def to_row(column, start):
    shape = (SEQS, LANES)
    picked = jnp.where(iota(shape, 1) == iota(shape, 0) + start, column, F32(0.0))
    return jnp.sum(picked, axis=0, keepdims=True)


def to_column(row, start):
    shape = (SEQS, LANES)
    picked = jnp.where(iota(shape, 1) == iota(shape, 0) + start, row, F32(0.0))
    return jnp.sum(picked, axis=1, keepdims=True)


def first_head():
    return iota((SEQS, LANES), 1) < HEAD_DIM


def per_head(values):
    low = jnp.sum(jnp.where(first_head(), values, F32(0.0)), axis=1, keepdims=True)
    high = jnp.sum(jnp.where(first_head(), F32(0.0), values), axis=1, keepdims=True)
    return low, high


def head_norm(values):
    low, high = per_head(values * values)
    return values * lax.rsqrt(jnp.where(first_head(), low, high) * (1.0 / HEAD_DIM) + eps)


def between(start, width):
    lane = iota((SEQS, LANES), 1)
    return (lane >= start) & (lane < start + width)


def row_of_slot(width):
    i = iota((1, width), 1)
    slot = (i * 7282) >> 16
    return slot, i - ROWS * slot


def prep(tokens, gain, w_query, w_key, w_value, w_gate, w_forget, logf, limits, slots):
    wide = tokens[...].astype(F32)
    squares = jnp.sum(wide * wide, axis=1, keepdims=True)
    scaled = wide * gain[...]

    def project(weight):
        return jnp.dot(scaled, weight[...].astype(F32), precision=HI, preferred_element_type=F32)

    forget = lax.dot_general(
        scaled, w_forget[...].astype(F32), NT, precision=HI, preferred_element_type=F32
    )
    live = iota((SEQS, SPAN), 1) < limits[...]
    row = to_row(squares, 0)
    for h in range(2):
        total = jnp.sum(jnp.where(live, logf[h], F32(0.0)), axis=1, keepdims=True)
        row = row + to_row(forget[:, h : h + 1], FORGET + SEQS * h)
        row = row + to_row(total, TOTAL + SEQS * h)
    query = project(w_query)
    parts = [project(w) for w in (w_key, w_value, w_gate)]
    for j in range(N_KV):
        slots[pl.ds(ROWS * j, SEQS), :] = query
    for c in range(8):
        tail = jnp.broadcast_to(row, (SEQS, LANES))
        for n, part in enumerate(parts):
            start = PIECES + PIECE * n
            moved = pltpu.roll(part, (start - PIECE * c) % LANES, 1)
            tail = jnp.where(between(start, PIECE), moved, tail)
        slots[pl.ds(ROWS * c + SEQS, SEQS, stride=ROWS * 8), :] = tail


def attend(slots, cache_key, cache_value, logf, limits, send, query_out, sums_out, shift_out):
    got = slots[...]
    width = N_KV * ROWS
    _, inside = row_of_slot(width)
    picks = (jnp.broadcast_to(inside, (16, width)) == iota((16, width), 0)).astype(F32)
    summed = jnp.dot(picks, got, precision=HI, preferred_element_type=F32)
    raw = summed[:SEQS]
    sums = summed[SEQS : SEQS + 1]
    inv_root = lax.rsqrt(to_column(sums, 0) * (1.0 / D) + eps)
    query = head_norm(raw * inv_root).astype(jnp.bfloat16)
    query_out[...] = query.astype(F32)
    sums_out[...] = jnp.broadcast_to(sums, (SEQS, LANES))

    tails = slots[pl.ds(SEQS, N_KV, stride=ROWS), :]
    shape = (N_KV, N_KV)
    upper = (iota(shape, 1) > iota(shape, 0)).astype(F32)
    shift_out[...] = jnp.dot(upper, tails, precision=HI, preferred_element_type=F32)

    blocks = []
    wide_query = query.astype(F32)
    seq = iota((SEQS, LANES), 0)
    for s in range(SEQS):
        mine = jnp.where(seq == s, wide_query, F32(0.0))
        low = jnp.where(first_head(), mine, F32(0.0))
        blocks.append(jnp.concatenate([low, mine - low], axis=0))
    spread = jnp.concatenate(blocks, axis=1).astype(jnp.bfloat16)
    keys = cache_key[...].reshape(SEQS * LANES, SPAN)
    scores = jnp.dot(spread, keys, preferred_element_type=F32) * HEAD_DIM ** (-0.5)

    live = iota((SEQS, SPAN), 1) < limits[...]
    live = jnp.concatenate([live.astype(F32), live.astype(F32)], axis=0) > 0.5
    gates = jnp.where(live, jnp.concatenate([logf[0], logf[1]], axis=0), F32(0.0))
    shape = (LANES, LANES)
    upper = (iota(shape, 0) > iota(shape, 1)).astype(F32)
    biases, after = [], jnp.zeros((2 * SEQS, 1), F32)
    for b in reversed(range(SPAN // LANES)):
        part = gates[:, LANES * b : LANES * (b + 1)]
        biases.append(jnp.dot(part, upper, precision=HI, preferred_element_type=F32) + after)
        after = after + jnp.sum(part, axis=1, keepdims=True)
    scores = scores + jnp.concatenate(biases[::-1], axis=1)
    peak = jnp.max(jnp.where(live, scores, F32(very_low)), axis=1, keepdims=True)
    weights = jnp.where(live, jnp.exp(scores - peak), F32(0.0))
    den = jnp.sum(weights, axis=1, keepdims=True)
    values = cache_value[...].reshape(SEQS * LANES, SPAN)
    crossed = lax.dot_general(
        weights.astype(jnp.bfloat16), values, NT, preferred_element_type=F32
    )
    local = jnp.zeros((SEQS, LANES), F32)
    for s in range(SEQS):
        block = crossed[:, LANES * s : LANES * (s + 1)]
        own = jnp.where(first_head(), block[:SEQS], block[SEQS:])
        local = jnp.where(seq == s, own, local)
    lane = iota((1, LANES), 1)
    row = jnp.where((lane >= PIECES) & (lane < PIECES + 3 * PIECE), sums, F32(0.0))
    for h in range(2):
        rows = slice(SEQS * h, SEQS * (h + 1))
        row = row + to_row(den[rows], SEQS * h) + to_row(peak[rows], TOTAL + SEQS * h)
    tail = jnp.broadcast_to(row, (SEQS, LANES))
    for j in range(N_KV):
        send[pl.ds(ROWS * j, SEQS), :] = local
    for c in range(8):
        send[pl.ds(ROWS * c + SEQS, SEQS, stride=ROWS * 8), :] = tail


def combine(slots, query, sums, shift, w_out, partial_out, key_out, value_out, logf_out):
    sums_row = sums[0:1, :]
    inv_root = lax.rsqrt(to_column(sums_row, 0) * (1.0 / D) + eps)
    parts = [jnp.zeros((SEQS, LANES), F32) for _ in range(3)]
    for c in range(8):
        tail = slots[pl.ds(ROWS * c + SEQS, SEQS, stride=ROWS * 8), :]
        for n in range(3):
            start = PIECES + PIECE * n
            moved = pltpu.roll(tail, (PIECE * c - start) % LANES, 1)
            parts[n] = jnp.where(between(PIECE * c, PIECE), moved, parts[n])
    key, value, gate = (part * inv_root for part in parts)
    key = head_norm(key).astype(jnp.bfloat16)
    key_out[...] = key
    value_out[...] = value
    score_new = [x * HEAD_DIM ** (-0.5) for x in per_head(query[...] * key.astype(F32))]
    tails = slots[pl.ds(SEQS, N_KV, stride=ROWS), :]
    logf_row = jnp.zeros((1, LANES), F32)
    score_row = jnp.zeros((1, LANES), F32)
    for h in range(2):
        forget = to_column(sums_row, FORGET + SEQS * h) * inv_root
        logf = jnp.minimum(forget, 0.0) - jnp.log1p(jnp.exp(-jnp.abs(forget)))
        logf_out[h] = jnp.broadcast_to(logf, (SEQS, LANES))
        logf_row = logf_row + to_row(logf, TOTAL + SEQS * h)
        score_row = score_row + to_row(score_new[h], TOTAL + SEQS * h)
    peaks = tails + shift[...] + logf_row
    peak = jnp.maximum(jnp.max(peaks, axis=0, keepdims=True), score_row)
    lane = iota((N_KV, LANES), 1)
    stats = (lane >= TOTAL) & (lane < TOTAL + 2 * SEQS)
    factors = jnp.where(stats, jnp.exp(jnp.where(stats, peaks - peak, F32(0.0))), F32(0.0))
    weight_new = jnp.exp(jnp.where(stats[0:1], score_row - peak, F32(0.0)))
    den = jnp.sum(factors * pltpu.roll(tails, TOTAL, 1), axis=0, keepdims=True) + weight_new
    width = N_KV * ROWS
    slot, inside = row_of_slot(width)
    expand = (jnp.broadcast_to(slot, (N_KV, width)) == iota((N_KV, width), 0)).astype(F32)
    turned = jnp.transpose(factors)[TOTAL : TOTAL + 2 * SEQS]
    wide = jnp.dot(turned, expand, precision=HI, preferred_element_type=F32)
    own = jnp.broadcast_to(inside, (2 * SEQS, width)) == (iota((2 * SEQS, width), 0) & 7)
    wide = jnp.where(own, wide, F32(0.0))
    both = jnp.dot(wide, slots[...], precision=HI, preferred_element_type=F32)
    low = first_head()
    weighted = jnp.where(low, both[:SEQS], both[SEQS:])

    def lanes_of(row):
        return jnp.where(low, to_column(row, TOTAL), to_column(row, TOTAL + SEQS))

    attended = (weighted + lanes_of(weight_new) * value) / lanes_of(den)
    silu = gate / (1.0 + jnp.exp(-gate))
    gated = (head_norm(attended) * silu).astype(jnp.bfloat16)
    mixed = jnp.zeros((SEQS, w_out.shape[1]), F32)
    for h in range(2):
        half = gated[:, HEAD_DIM * h : HEAD_DIM * (h + 1)]
        mixed = mixed + lax.dot_general(half, w_out[h], NT, preferred_element_type=F32)
    partial_out[...] = mixed


def exchange(slots):
    slots = lax.all_to_all(slots.reshape(N_KV, 1, ROWS * LANES), KV, 0, 0, tiled=True)
    return slots.reshape(N_KV * ROWS, LANES)


def call(kernel, name, *outs):
    shapes = [jax.ShapeDtypeStruct(shape, dtype) for shape, dtype in outs]
    params = pltpu.CompilerParams(vmem_limit_bytes=VMEM)
    return pl.pallas_call(kernel, out_shape=shapes, name=name, compiler_params=params)


def on_device(
    tokens,
    norm_gain,
    w_query,
    w_key,
    w_value,
    w_gate,
    w_forget,
    w_out,
    cache_key,
    cache_value,
    cache_logf,
    lengths,
):
    model = tokens.shape[1]
    limits = (lengths - lax.axis_index(KV) * SPAN)[:, None]
    flat = [w.reshape(model, LANES) for w in (w_query, w_key, w_value, w_gate)]
    logf = jnp.transpose(cache_logf, (2, 0, 1))
    whole = (N_KV * ROWS, LANES)
    tile = (SEQS, LANES)
    (first,) = call(prep, "prep", (whole, F32))(
        tokens, norm_gain[None, :], *flat, jnp.transpose(w_forget), logf, limits
    )
    first = exchange(first)
    second, query, sums, shift = call(
        attend, "attend", (whole, F32), (tile, F32), (tile, F32), ((N_KV, LANES), F32)
    )(
        first,
        jnp.transpose(cache_key, (0, 2, 3, 1)),
        jnp.transpose(cache_value, (0, 2, 3, 1)),
        logf,
        limits,
    )
    second = exchange(second)
    partial_out, key_new, value_new, logf_new = call(
        combine,
        "combine",
        ((SEQS, model), F32),
        (tile, jnp.bfloat16),
        (tile, F32),
        ((2,) + tile, F32),
    )(second, query, sums, shift, jnp.transpose(w_out, (0, 2, 1)))
    mixed = lax.all_gather(partial_out, "tp").sum(0)
    heads = (SEQS, 2, HEAD_DIM)
    return (
        mixed,
        key_new.reshape(heads),
        value_new.reshape(heads),
        jnp.transpose(logf_new[:, :, 0]),
    )


def solution(mesh):
    finer = Mesh(
        mesh.devices.reshape(mesh.shape["dp"], 8, 8, mesh.shape["tp"]), ("dp", "kv_0", "kv_1", "tp")
    )
    return jax.shard_map(
        on_device,
        mesh=finer,
        in_specs=(
            P("dp", KV),
            P(KV),
            P(KV, "tp", None),
            P(KV, "tp", None),
            P(KV, "tp", None),
            P(KV, "tp", None),
            P(KV, "tp"),
            P("tp", None, KV),
            P("dp", KV, "tp", None),
            P("dp", KV, "tp", None),
            P("dp", KV, "tp"),
            P("dp"),
        ),
        out_specs=(P("dp", KV), P("dp", "tp", None), P("dp", "tp", None), P("dp", "tp")),
        check_vma=False,
    )
```

time: 79.4 us -> 68.9 us (0.87)
  waiting for transfers between devices: 16.3 us -> 0 us
  blocking collectives: 40.2 us -> 53.8 us
  starting transfers between devices: 6.62 us -> 0 us
  Pallas kernels: 0 us -> 2.62 us
  other arithmetic: 3.59 us -> 1.34 us
  matrix products: 1.89 us -> 0 us
    all_to_all x1 -> x0, waiting for transfers between devices: 16.3 us -> none  [exchange(): return lax.all_to_all(slots, KV, 0, 0, tiled=True)]
    all_to_all x1 -> x2, blocking collectives: 34.9 us -> 48.4 us  [exchange(): lax.all_to_all(slots.reshape(N_KV, 1, ROWS * LANES), KV, 0, 0, tiled=True)]
    all_to_all x1 -> x0, starting transfers between devices: 6.62 us -> none  [exchange(): return lax.all_to_all(slots, KV, 0, 0, tiled=True)]
    reshape x15 -> x6, local copies, waits for them, and re-layouts: 1.23 us -> 4.46 us  [the longest x4 3.12 us: on_device(): flat = [w.reshape(model, LANES) for w in (w_query, w_key, w_value, w_gate)]]
    pallas_call x0 -> x3, Pallas kernels: none -> 2.62 us  [the longest x1 1.31 us: on_device(): call(attend, 'attend', (whole, F32), (tile, F32), (tile, F32), ((N_KV, LA...]
    reduce_sum x9 -> x0, other arithmetic: 2.28 us -> none  [the longest x3 1 us: head_norm(): jnp.mean(values * values, axis=-1, keepdims=True) + eps]
    dot_general x10 -> x0, matrix products: 1.89 us -> none  [the longest x5 0.59 us: project(): jnp.dot(scaled, weight.reshape(weight.shape[0], -1).astype(jnp.float32),...]
    broadcast_in_dim x7 -> x1, local copies, waits for them, and re-layouts: 1.03 us -> 0.08 us  [on_device(): limits = (lengths - lax.axis_index(KV) * SPAN)[:, None]]
  transfers between devices with their start and end apart: 1 -> 0, of which waited for: 1 -> 0; matrix products, arithmetic and copies ran while one was open for 1% -> 0% of each run, Pallas kernels for 0% -> 0%
where the time goes in v2:
time: 68.9 us; the launch traced here: 68.3 us
  blocking collectives  53.8 us (78%)
  local copies, waits for them, and re-layouts  9.9 us (14%)
  Pallas kernels  2.62 us (4%)
  other arithmetic  1.34 us (2%)
    all_to_all x2, blocking collectives, exchange(): lax.all_to_all(slots.reshape(N_KV, 1, ROWS * LANES), KV, 0, 0, tiled=True)  48.4 us
    all_gather x1, blocking collectives, on_device(): mixed = lax.all_gather(partial_out, 'tp').sum(0)  5.34 us
    unnamed x13, local copies, waits for them, and re-layouts  4.68 us
    reshape x4, local copies, waits for them, and re-layouts, on_device(): flat = [w.reshape(model, LANES) for w in (w_query, w_key, w_value, w_gate)]  3.12 us

profile of v2, /device:TPU:1, one launch (start us, length us, event | category | flops | bytes accessed | tf_op | source)
XLA Modules:
  0.0 68.3 jit_solution(17479396396159513792)
XLA Ops:
  0.6 0.0 copy-start
  0.6 0.7 %subtract_bitcast_fusion = s32[8,1]{0,1:T(1,128)S(1)} fusion(s32[8]{0:T(128)} %param.23, s32[]{:T(128)S(6)} %mul.7), kind=kLoop, calls=%fused_computation.3 | loop fusion | flops 8 | bytes 68 | tf_op jit(solution)/shard_map/broadcast_in_dim | solution.py:245
  1.4 0.1 copy.23.limits
  1.5 0.8 %reshape.38.w_query = bf16[16,128]{1,0:T(8,128)(2,1)S(1)} reshape(bf16[16,2,64]{2,1,0:T(2,128)(2,1)} %param.14) | data formatting | bytes 8192 | tf_op jit(solution)/shard_map/reshape | solution.py:246
  2.3 0.8 %reshape.39.w_key = bf16[16,128]{1,0:T(8,128)(2,1)S(1)} reshape(bf16[16,2,64]{2,1,0:T(2,128)(2,1)} %param.15) | data formatting | bytes 8192 | tf_op jit(solution)/shard_map/reshape | solution.py:246
  3.0 0.8 %reshape.40.w_value = bf16[16,128]{1,0:T(8,128)(2,1)S(1)} reshape(bf16[16,2,64]{2,1,0:T(2,128)(2,1)} %param.16) | data formatting | bytes 8192 | tf_op jit(solution)/shard_map/reshape | solution.py:246
  3.8 0.8 %reshape.41.w_gate = bf16[16,128]{1,0:T(8,128)(2,1)S(1)} reshape(bf16[16,2,64]{2,1,0:T(2,128)(2,1)} %param.17) | data formatting | bytes 8192 | tf_op jit(solution)/shard_map/reshape | solution.py:246
  4.6 0.8 %copy.28 = f32[8,512,2]{1,0,2:T(8,128)S(1)} copy(f32[8,512,2]{1,2,0:T(2,128)} %param.22) | data formatting | bytes 65536 | tf_op args[10]
  5.4 0.0 copy-start.3
  5.4 0.7 copy-done.3
  6.0 0.0 copy-start.4
  6.1 0.7 copy-done.4
  6.7 0.0 copy-start.5
  6.7 0.7 copy-done.5
  7.4 0.3 prep.1
  7.6 30.8 %all_to_all.10 = f32[64,1,1152]{2,1,0:T(1,128)S(1)} all-to-all(f32[64,1,1152]{2,1,0:T(1,128)S(1)} %bitcast.19), channel_id=1, replica_groups=mesh['dp'=4,'kv_0'=8,'kv_1'=8,'tp'=2] {'kv_0','kv_1'}, dimensions={0} | all-to-all | bytes 589824 | tf_op jit(solution)/shard_map/all_to_all | solution.py:220
  38.5 0.0 copy-done
  38.5 0.0 copy-start.1
  38.5 1.2 %copy-done.1 = bf16[8,512,2,64]{1,3,2,0:T(8,128)(2,1)S(1)} copy-done((bf16[8,512,2,64]{1,3,2,0:T(8,128)(2,1)S(1)}, bf16[8,512,2,64]{1,3,2,0:T(8,128)(2,1)}, u32[]{:S(2)}) %copy-start.1) | copy-done | bytes 1048600
  39.7 1.3 %attend.1 = (f32[576,128]{1,0:T(8,128)S(1)}, f32[8,128]{1,0:T(8,128)S(1)}, f32[8,128]{1,0:T(8,128)S(1)}, f32[64,128]{1,0:T(8,128)S(1)}) custom-call(f32[576,128]{1,0:T(8,128)S(1)} %bitcast.17, bf16[8,2,64,512]{3,2,1,0:T(8,128)(2,1)S(1)} %bitcast.20, bf16[8,2,64,512]{3,2,1,0:T(8,128)(2,1)S(1)} %bitcast.21, f32[2,8,512]{2,1,0:T(8,128)S(1)} %bitcast.23, ...), custom_call_target="tpu_custom_call" | custom-call | tf_op jit(solution)/shard_map/attend/pallas_call | solution.py:254
  41.0 17.6 %all_to_all.11 = f32[64,1,1152]{2,1,0:T(1,128)S(1)} all-to-all(f32[64,1,1152]{2,1,0:T(1,128)S(1)} %bitcast.24), channel_id=1, replica_groups=mesh['dp'=4,'kv_0'=8,'kv_1'=8,'tp'=2] {'kv_0','kv_1'}, dimensions={0} | all-to-all | bytes 589824 | tf_op jit(solution)/shard_map/all_to_all | solution.py:220
  58.6 0.0 copy-start.2
  58.6 0.7 %copy-done.2 = bf16[2,64,16]{1,2,0:T(8,128)(2,1)S(1)} copy-done((bf16[2,64,16]{1,2,0:T(8,128)(2,1)S(1)}, bf16[2,64,16]{1,2,0:T(8,128)(2,1)}, u32[]{:S(2)}) %copy-start.2) | copy-done | bytes 4120
  59.3 1.0 %combine.1 = (f32[8,16]{1,0:T(8,128)S(1)}, bf16[8,128]{1,0:T(8,128)(2,1)S(1)}, f32[8,128]{1,0:T(8,128)S(1)}, f32[2,8,128]{2,1,0:T(8,128)S(1)}) custom-call(f32[576,128]{1,0:T(8,128)S(1)} %bitcast.18, f32[8,128]{1,0:T(8,128)S(1)} %get-tuple-element.13.query, f32[8,128]{1,0:T(8,128)S(1)} %get-tuple-element.14.sums, f32[64,128]{1,0:T(8,128)S(1)} %get-tuple-element.15.shift, ...), custom_call_target="tpu_custom_call" | custom-call | tf_op jit(solution)/shard_map/combine/pallas_call | solution.py:264
  60.4 0.7 slice_reduce_fusion
  61.0 5.3 %all-gather = f32[16,16]{1,0:T(8,128)S(1)} all-gather(f32[8,16]{1,0:T(8,128)S(1)} %get-tuple-element.16), channel_id=2, replica_groups=mesh['dp'=4,'kv_0'=8,'kv_1'=8,'tp'=2] {'tp'}, dimensions={0}, use_global_device_ids=true | all-gather | bytes 1536 | tf_op jit(solution)/shard_map/all_gather | solution.py:272
  66.4 0.6 bitcast_reduce_fusion
  67.0 0.7 reshape.46
  67.7 0.7 reshape.47
Async XLA Ops:
  0.6 37.8 %copy-start = (bf16[8,512,2,64]{1,3,2,0:T(8,128)(2,1)S(1)}, bf16[8,512,2,64]{1,3,2,0:T(8,128)(2,1)}, u32[]{:S(2)}) copy-start(bf16[8,512,2,64]{1,3,2,0:T(8,128)(2,1)} %param.20) | copy-start | bytes 3145732
  5.4 0.7 copy-start.3
  6.0 0.7 copy-start.4
  6.7 0.7 copy-start.5
  38.5 1.2 %copy-start.1 = (bf16[8,512,2,64]{1,3,2,0:T(8,128)(2,1)S(1)}, bf16[8,512,2,64]{1,3,2,0:T(8,128)(2,1)}, u32[]{:S(2)}) copy-start(bf16[8,512,2,64]{1,3,2,0:T(8,128)(2,1)} %param.21) | copy-start | bytes 3145732
  58.6 0.7 %copy-start.2 = (bf16[2,64,16]{1,2,0:T(8,128)(2,1)S(1)}, bf16[2,64,16]{1,2,0:T(8,128)(2,1)}, u32[]{:S(2)}) copy-start(bf16[2,64,16]{1,2,0:T(8,128)(2,1)} %param.19) | copy-start | bytes 12292

commit v3 on v2

--- a/solution.py
+++ b/solution.py
@@ -67,23 +67,51 @@
     return slot, i - ROWS * slot
 
 
-def prep(tokens, gain, w_query, w_key, w_value, w_gate, w_forget, logf, limits, slots):
+def prep(*refs):
+    sources, (slots, bias_out, keys, values, w_out, *local, sems) = refs[:12], refs[12:]
+    targets = (*local, keys, values, w_out)
+    copies = [
+        pltpu.make_async_copy(source, target, sems.at[n])
+        for n, (source, target) in enumerate(zip(sources, targets))
+    ]
+    for copy in copies:
+        copy.start()
+    for copy in copies[:9]:
+        copy.wait()
+    tokens, gain, w_query, w_key, w_value, w_gate, w_forget, logf, lengths = local
     wide = tokens[...].astype(F32)
     squares = jnp.sum(wide * wide, axis=1, keepdims=True)
     scaled = wide * gain[...]
 
     def project(weight):
-        return jnp.dot(scaled, weight[...].astype(F32), precision=HI, preferred_element_type=F32)
+        weight = weight[...].astype(F32)
+        halves = [
+            jnp.dot(scaled, weight[:, h, :], precision=HI, preferred_element_type=F32)
+            for h in range(2)
+        ]
+        return jnp.concatenate(halves, axis=1)
 
     forget = lax.dot_general(
         scaled, w_forget[...].astype(F32), NT, precision=HI, preferred_element_type=F32
     )
-    live = iota((SEQS, SPAN), 1) < limits[...]
+    shard = lax.axis_index("kv_0") * 8 + lax.axis_index("kv_1")
+    limits = jnp.where(iota((SEQS, SEQS), 0) == iota((SEQS, SEQS), 1), lengths[...], 0)
+    limits = jnp.sum(limits, axis=1, keepdims=True) - shard * SPAN
+    live = iota((SEQS, SPAN), 1) < limits
+    shape = (LANES, LANES)
+    upper = (iota(shape, 0) > iota(shape, 1)).astype(F32)
     row = to_row(squares, 0)
     for h in range(2):
-        total = jnp.sum(jnp.where(live, logf[h], F32(0.0)), axis=1, keepdims=True)
+        gates = jnp.where(live, logf[:, h, :], F32(0.0))
+        biases, after = [], jnp.zeros((SEQS, 1), F32)
+        for b in reversed(range(SPAN // LANES)):
+            part = gates[:, LANES * b : LANES * (b + 1)]
+            biases.append(jnp.dot(part, upper, precision=HI, preferred_element_type=F32) + after)
+            after = after + jnp.sum(part, axis=1, keepdims=True)
+        bias = jnp.concatenate(biases[::-1], axis=1)
+        bias_out[pl.ds(SEQS * h, SEQS), :] = jnp.where(live, bias, F32(very_low))
         row = row + to_row(forget[:, h : h + 1], FORGET + SEQS * h)
-        row = row + to_row(total, TOTAL + SEQS * h)
+        row = row + to_row(after, TOTAL + SEQS * h)
     query = project(w_query)
     parts = [project(w) for w in (w_key, w_value, w_gate)]
     for j in range(N_KV):
@@ -95,9 +123,13 @@
             moved = pltpu.roll(part, (start - PIECE * c) % LANES, 1)
             tail = jnp.where(between(start, PIECE), moved, tail)
         slots[pl.ds(ROWS * c + SEQS, SEQS, stride=ROWS * 8), :] = tail
-
-
-def attend(slots, cache_key, cache_value, logf, limits, send, query_out, sums_out, shift_out):
+    for copy in copies[9:]:
+        copy.wait()
+
+
+def attend(
+    slots, cache_key, cache_value, bias, send, query_out, sums_out, shift_out, logf_out
+):
     got = slots[...]
     width = N_KV * ROWS
     _, inside = row_of_slot(width)
@@ -110,10 +142,17 @@
     query_out[...] = query.astype(F32)
     sums_out[...] = jnp.broadcast_to(sums, (SEQS, LANES))
 
+    logf_row = jnp.zeros((1, LANES), F32)
+    for h in range(2):
+        forget = to_column(sums, FORGET + SEQS * h) * inv_root
+        logf = jnp.minimum(forget, 0.0) - jnp.log1p(jnp.exp(-jnp.abs(forget)))
+        logf_out[pl.ds(h, 1), :] = to_row(logf, 0)[:, :SEQS]
+        logf_row = logf_row + to_row(logf, TOTAL + SEQS * h)
     tails = slots[pl.ds(SEQS, N_KV, stride=ROWS), :]
     shape = (N_KV, N_KV)
     upper = (iota(shape, 1) > iota(shape, 0)).astype(F32)
-    shift_out[...] = jnp.dot(upper, tails, precision=HI, preferred_element_type=F32)
+    later = jnp.dot(upper, tails, precision=HI, preferred_element_type=F32)
+    shift_out[...] = later + logf_row
 
     blocks = []
     wide_query = query.astype(F32)
@@ -126,18 +165,9 @@
     keys = cache_key[...].reshape(SEQS * LANES, SPAN)
     scores = jnp.dot(spread, keys, preferred_element_type=F32) * HEAD_DIM ** (-0.5)
 
-    live = iota((SEQS, SPAN), 1) < limits[...]
-    live = jnp.concatenate([live.astype(F32), live.astype(F32)], axis=0) > 0.5
-    gates = jnp.where(live, jnp.concatenate([logf[0], logf[1]], axis=0), F32(0.0))
-    shape = (LANES, LANES)
-    upper = (iota(shape, 0) > iota(shape, 1)).astype(F32)
-    biases, after = [], jnp.zeros((2 * SEQS, 1), F32)
-    for b in reversed(range(SPAN // LANES)):
-        part = gates[:, LANES * b : LANES * (b + 1)]
-        biases.append(jnp.dot(part, upper, precision=HI, preferred_element_type=F32) + after)
-        after = after + jnp.sum(part, axis=1, keepdims=True)
-    scores = scores + jnp.concatenate(biases[::-1], axis=1)
-    peak = jnp.max(jnp.where(live, scores, F32(very_low)), axis=1, keepdims=True)
+    live = bias[...] > F32(0.5 * very_low)
+    scores = jnp.where(live, scores + bias[...], F32(very_low))
+    peak = jnp.max(scores, axis=1, keepdims=True)
     weights = jnp.where(live, jnp.exp(scores - peak), F32(0.0))
     den = jnp.sum(weights, axis=1, keepdims=True)
     values = cache_value[...].reshape(SEQS * LANES, SPAN)
@@ -161,7 +191,7 @@
         send[pl.ds(ROWS * c + SEQS, SEQS, stride=ROWS * 8), :] = tail
 
 
-def combine(slots, query, sums, shift, w_out, partial_out, key_out, value_out, logf_out):
+def combine(slots, query, sums, shift, w_out, partial_out, key_out, value_out):
     sums_row = sums[0:1, :]
     inv_root = lax.rsqrt(to_column(sums_row, 0) * (1.0 / D) + eps)
     parts = [jnp.zeros((SEQS, LANES), F32) for _ in range(3)]
@@ -173,19 +203,16 @@
             parts[n] = jnp.where(between(PIECE * c, PIECE), moved, parts[n])
     key, value, gate = (part * inv_root for part in parts)
     key = head_norm(key).astype(jnp.bfloat16)
-    key_out[...] = key
-    value_out[...] = value
+    for h in range(2):
+        part = slice(HEAD_DIM * h, HEAD_DIM * (h + 1))
+        key_out[:, h, :] = key[:, part]
+        value_out[:, h, :] = value[:, part]
     score_new = [x * HEAD_DIM ** (-0.5) for x in per_head(query[...] * key.astype(F32))]
     tails = slots[pl.ds(SEQS, N_KV, stride=ROWS), :]
-    logf_row = jnp.zeros((1, LANES), F32)
     score_row = jnp.zeros((1, LANES), F32)
     for h in range(2):
-        forget = to_column(sums_row, FORGET + SEQS * h) * inv_root
-        logf = jnp.minimum(forget, 0.0) - jnp.log1p(jnp.exp(-jnp.abs(forget)))
-        logf_out[h] = jnp.broadcast_to(logf, (SEQS, LANES))
-        logf_row = logf_row + to_row(logf, TOTAL + SEQS * h)
         score_row = score_row + to_row(score_new[h], TOTAL + SEQS * h)
-    peaks = tails + shift[...] + logf_row
+    peaks = tails + shift[...]
     peak = jnp.maximum(jnp.max(peaks, axis=0, keepdims=True), score_row)
     lane = iota((N_KV, LANES), 1)
     stats = (lane >= TOTAL) & (lane < TOTAL + 2 * SEQS)
@@ -221,10 +248,11 @@
     return slots.reshape(N_KV * ROWS, LANES)
 
 
-def call(kernel, name, *outs):
+def call(kernel, name, outs, operands, **more):
     shapes = [jax.ShapeDtypeStruct(shape, dtype) for shape, dtype in outs]
     params = pltpu.CompilerParams(vmem_limit_bytes=VMEM)
-    return pl.pallas_call(kernel, out_shape=shapes, name=name, compiler_params=params)
+    run = pl.pallas_call(kernel, out_shape=shapes, name=name, compiler_params=params, **more)
+    return run(*operands)
 
 
 def on_device(
@@ -241,42 +269,36 @@
     cache_logf,
     lengths,
 ):
-    model = tokens.shape[1]
-    limits = (lengths - lax.axis_index(KV) * SPAN)[:, None]
-    flat = [w.reshape(model, LANES) for w in (w_query, w_key, w_value, w_gate)]
-    logf = jnp.transpose(cache_logf, (2, 0, 1))
-    whole = (N_KV * ROWS, LANES)
-    tile = (SEQS, LANES)
-    (first,) = call(prep, "prep", (whole, F32))(
-        tokens, norm_gain[None, :], *flat, jnp.transpose(w_forget), logf, limits
-    )
-    first = exchange(first)
-    second, query, sums, shift = call(
-        attend, "attend", (whole, F32), (tile, F32), (tile, F32), ((N_KV, LANES), F32)
-    )(
-        first,
-        jnp.transpose(cache_key, (0, 2, 3, 1)),
-        jnp.transpose(cache_value, (0, 2, 3, 1)),
-        logf,
-        limits,
-    )
-    second = exchange(second)
-    partial_out, key_new, value_new, logf_new = call(
+    whole = ((N_KV * ROWS, LANES), F32)
+    tile = ((SEQS, LANES), F32)
+    small = (tokens, norm_gain[None, :], w_query, w_key, w_value, w_gate, jnp.transpose(w_forget))
+    small = small + (jnp.transpose(cache_logf, (0, 2, 1)), lengths[None, :])
+    large = [jnp.transpose(cache, (0, 2, 3, 1)) for cache in (cache_key, cache_value)]
+    large.append(jnp.transpose(w_out, (0, 2, 1)))
+    first, bias, keys, values, w_out = call(
+        prep,
+        "prep",
+        [whole, ((2 * SEQS, SPAN), F32)] + [(x.shape, x.dtype) for x in large],
+        [pltpu.with_memory_space_constraint(x, pltpu.HBM) for x in (*small, *large)],
+        in_specs=[pl.BlockSpec(memory_space=pltpu.HBM)] * 12,
+        scratch_shapes=[pltpu.VMEM(x.shape, x.dtype) for x in small]
+        + [pltpu.SemaphoreType.DMA((12,))],
+    )
+    second, query, sums, shift, logf_new = call(
+        attend,
+        "attend",
+        [whole, tile, tile, ((N_KV, LANES), F32), ((2, SEQS), F32)],
+        (exchange(first), keys, values, bias),
+    )
+    heads = (SEQS, 2, HEAD_DIM)
+    partial_out, key_new, value_new = call(
         combine,
         "combine",
-        ((SEQS, model), F32),
-        (tile, jnp.bfloat16),
-        (tile, F32),
-        ((2,) + tile, F32),
-    )(second, query, sums, shift, jnp.transpose(w_out, (0, 2, 1)))
+        [((SEQS, tokens.shape[1]), F32), (heads, jnp.bfloat16), (heads, F32)],
+        (exchange(second), query, sums, shift, w_out),
+    )
     mixed = lax.all_gather(partial_out, "tp").sum(0)
-    heads = (SEQS, 2, HEAD_DIM)
-    return (
-        mixed,
-        key_new.reshape(heads),
-        value_new.reshape(heads),
-        jnp.transpose(logf_new[:, :, 0]),
-    )
+    return mixed, key_new, value_new, jnp.transpose(logf_new)
 
 
 def solution(mesh):

time: 68.9 us -> 60 us (0.87)
  local copies, waits for them, and re-layouts: 9.9 us -> 0 us
  Pallas kernels: 2.62 us -> 4.78 us
  other arithmetic: 1.34 us -> 0.6 us
    unnamed x13 -> x0, local copies, waits for them, and re-layouts: 4.68 us -> none
    reshape x6 -> x0, local copies, waits for them, and re-layouts: 4.46 us -> none  [the longest x4 3.12 us: on_device(): flat = [w.reshape(model, LANES) for w in (w_query, w_key, w_value, w_gate)]]
    pallas_call x3, Pallas kernels: 2.62 us -> 4.78 us  [call(): return run(*operands)]
    broadcast_in_dim x1 -> x0, other arithmetic: 0.75 us -> none  [on_device(): limits = (lengths - lax.axis_index(KV) * SPAN)[:, None]]
where the time goes in v3:
time: 60 us; the launch traced here: 59.8 us
  blocking collectives  53.8 us (90%)
  Pallas kernels  4.78 us (8%)
  between operations  0.65 us (1%)
  other arithmetic  0.6 us (1%)
    all_to_all x2, blocking collectives, exchange(): lax.all_to_all(slots.reshape(N_KV, 1, ROWS * LANES), KV, 0, 0, tiled=True)  48.4 us
    all_gather x1, blocking collectives, on_device(): mixed = lax.all_gather(partial_out, 'tp').sum(0)  5.34 us
    pallas_call x3, Pallas kernels, call(): return run(*operands)  4.78 us

profile of v3, /device:TPU:1, one launch (start us, length us, event | category | flops | bytes accessed | tf_op | source)
XLA Modules:
  0.0 59.8 jit_solution(17295852408813936630)
XLA Ops:
  0.6 1.9 %prep.1 = (f32[576,128]{1,0:T(8,128)S(1)}, f32[16,512]{1,0:T(8,128)S(1)}, bf16[8,2,64,512]{3,2,1,0:T(8,128)(2,1)S(1)}, bf16[8,2,64,512]{3,2,1,0:T(8,128)(2,1)S(1)}, bf16[2,16,64]{2,1,0:T(8,128)(2,1)S(1)}) custom-call(bf16[8,16]{1,0:T(8,128)(2,1)} %refs_0_.1, f32[1,16]{1,0:T(1,128)} %bitcast.22, bf16[16,2,64]{2,1,0:T(2,128)(2,1)} %refs_2_.1, ...), custom_call_target="tpu_custom_call" | custom-call | tf_op jit(solution)/shard_map/prep/pallas_call | solution.py:255
  2.5 30.8 %all_to_all.10 = f32[64,1,1152]{2,1,0:T(1,128)S(1)} all-to-all(f32[64,1,1152]{2,1,0:T(1,128)S(1)} %bitcast.17), channel_id=1, replica_groups=mesh['dp'=4,'kv_0'=8,'kv_1'=8,'tp'=2] {'kv_0','kv_1'}, dimensions={0} | all-to-all | bytes 589824 | tf_op jit(solution)/shard_map/all_to_all | solution.py:247
  33.3 1.4 %attend.1 = (f32[576,128]{1,0:T(8,128)S(1)}, f32[8,128]{1,0:T(8,128)S(1)}, f32[8,128]{1,0:T(8,128)S(1)}, f32[64,128]{1,0:T(8,128)S(1)}, f32[2,8]{1,0:T(2,128)}) custom-call(f32[576,128]{1,0:T(8,128)S(1)} %bitcast.14, bf16[8,2,64,512]{3,2,1,0:T(8,128)(2,1)S(1)} %get-tuple-element.18.cache_key, bf16[8,2,64,512]{3,2,1,0:T(8,128)(2,1)S(1)} %get-tuple-element.19.cache_value, ...), custom_call_target="tpu_custom_call" | custom-call | tf_op jit(solution)/shard_map/attend/pallas_call | solution.py:255
  34.7 17.6 %all_to_all.11 = f32[64,1,1152]{2,1,0:T(1,128)S(1)} all-to-all(f32[64,1,1152]{2,1,0:T(1,128)S(1)} %bitcast.16), channel_id=1, replica_groups=mesh['dp'=4,'kv_0'=8,'kv_1'=8,'tp'=2] {'kv_0','kv_1'}, dimensions={0} | all-to-all | bytes 589824 | tf_op jit(solution)/shard_map/all_to_all | solution.py:247
  52.3 1.6 %combine.1 = (f32[8,16]{1,0:T(8,128)S(1)}, bf16[8,2,64]{2,1,0:T(2,128)(2,1)}, f32[8,2,64]{2,1,0:T(2,128)}) custom-call(f32[576,128]{1,0:T(8,128)S(1)} %bitcast.15, f32[8,128]{1,0:T(8,128)S(1)} %get-tuple-element.22.query, f32[8,128]{1,0:T(8,128)S(1)} %get-tuple-element.23.sums, f32[64,128]{1,0:T(8,128)S(1)} %get-tuple-element.24.shift, ...), custom_call_target="tpu_custom_call" | custom-call | tf_op jit(solution)/shard_map/combine/pallas_call | solution.py:255
  53.9 5.3 %all-gather = f32[16,16]{1,0:T(8,128)S(1)} all-gather(f32[8,16]{1,0:T(8,128)S(1)} %get-tuple-element.26), channel_id=2, replica_groups=mesh['dp'=4,'kv_0'=8,'kv_1'=8,'tp'=2] {'tp'}, dimensions={0}, use_global_device_ids=true | all-gather | bytes 1536 | tf_op jit(solution)/shard_map/all_gather | solution.py:300
  59.2 0.6 bitcast_reduce_fusion

commit v4 on v3

--- a/solution.py
+++ b/solution.py
@@ -61,10 +61,22 @@
     return (lane >= start) & (lane < start + width)
 
 
-def row_of_slot(width):
-    i = iota((1, width), 1)
-    slot = (i * 7282) >> 16
-    return slot, i - ROWS * slot
+def rows_at(start):
+    return pl.ds(start, SEQS, stride=ROWS)
+
+
+def fill(slots, values):
+    for s in range(SEQS):
+        row = jnp.broadcast_to(values[s : s + 1, :], (SEQS, LANES))
+        for g in range(N_KV // SEQS):
+            slots[rows_at(ROWS * SEQS * g + s), :] = row
+
+
+def total_row(slots, r):
+    parts = [slots[rows_at(ROWS * SEQS * g + r), :] for g in range(N_KV // SEQS)]
+    while len(parts) > 1:
+        parts = [a + b for a, b in zip(parts[::2], parts[1::2])]
+    return jnp.sum(parts[0], axis=0, keepdims=True)
 
 
 def prep(*refs):
@@ -114,8 +126,7 @@
         row = row + to_row(after, TOTAL + SEQS * h)
     query = project(w_query)
     parts = [project(w) for w in (w_key, w_value, w_gate)]
-    for j in range(N_KV):
-        slots[pl.ds(ROWS * j, SEQS), :] = query
+    fill(slots, query)
     for c in range(8):
         tail = jnp.broadcast_to(row, (SEQS, LANES))
         for n, part in enumerate(parts):
@@ -130,13 +141,11 @@
 def attend(
     slots, cache_key, cache_value, bias, send, query_out, sums_out, shift_out, logf_out
 ):
-    got = slots[...]
-    width = N_KV * ROWS
-    _, inside = row_of_slot(width)
-    picks = (jnp.broadcast_to(inside, (16, width)) == iota((16, width), 0)).astype(F32)
-    summed = jnp.dot(picks, got, precision=HI, preferred_element_type=F32)
-    raw = summed[:SEQS]
-    sums = summed[SEQS : SEQS + 1]
+    seq = iota((SEQS, LANES), 0)
+    raw = jnp.zeros((SEQS, LANES), F32)
+    for s in range(SEQS):
+        raw = jnp.where(seq == s, total_row(slots, s), raw)
+    sums = total_row(slots, SEQS)
     inv_root = lax.rsqrt(to_column(sums, 0) * (1.0 / D) + eps)
     query = head_norm(raw * inv_root).astype(jnp.bfloat16)
     query_out[...] = query.astype(F32)
@@ -156,7 +165,6 @@
 
     blocks = []
     wide_query = query.astype(F32)
-    seq = iota((SEQS, LANES), 0)
     for s in range(SEQS):
         mine = jnp.where(seq == s, wide_query, F32(0.0))
         low = jnp.where(first_head(), mine, F32(0.0))
@@ -185,8 +193,7 @@
         rows = slice(SEQS * h, SEQS * (h + 1))
         row = row + to_row(den[rows], SEQS * h) + to_row(peak[rows], TOTAL + SEQS * h)
     tail = jnp.broadcast_to(row, (SEQS, LANES))
-    for j in range(N_KV):
-        send[pl.ds(ROWS * j, SEQS), :] = local
+    fill(send, local)
     for c in range(8):
         send[pl.ds(ROWS * c + SEQS, SEQS, stride=ROWS * 8), :] = tail
 
@@ -219,16 +226,17 @@
     factors = jnp.where(stats, jnp.exp(jnp.where(stats, peaks - peak, F32(0.0))), F32(0.0))
     weight_new = jnp.exp(jnp.where(stats[0:1], score_row - peak, F32(0.0)))
     den = jnp.sum(factors * pltpu.roll(tails, TOTAL, 1), axis=0, keepdims=True) + weight_new
-    width = N_KV * ROWS
-    slot, inside = row_of_slot(width)
-    expand = (jnp.broadcast_to(slot, (N_KV, width)) == iota((N_KV, width), 0)).astype(F32)
-    turned = jnp.transpose(factors)[TOTAL : TOTAL + 2 * SEQS]
-    wide = jnp.dot(turned, expand, precision=HI, preferred_element_type=F32)
-    own = jnp.broadcast_to(inside, (2 * SEQS, width)) == (iota((2 * SEQS, width), 0) & 7)
-    wide = jnp.where(own, wide, F32(0.0))
-    both = jnp.dot(wide, slots[...], precision=HI, preferred_element_type=F32)
-    low = first_head()
-    weighted = jnp.where(low, both[:SEQS], both[SEQS:])
+    low, seq = first_head(), iota((SEQS, LANES), 0)
+    weighted = jnp.zeros((SEQS, LANES), F32)
+    for s in range(SEQS):
+        sums_of = []
+        for g in range(N_KV // SEQS):
+            own = factors[SEQS * g : SEQS * (g + 1)]
+            first, second = (own[:, n : n + 1] for n in (TOTAL + s, TOTAL + SEQS + s))
+            sums_of.append(jnp.where(low, first, second) * slots[rows_at(ROWS * SEQS * g + s), :])
+        while len(sums_of) > 1:
+            sums_of = [a + b for a, b in zip(sums_of[::2], sums_of[1::2])]
+        weighted = jnp.where(seq == s, jnp.sum(sums_of[0], axis=0, keepdims=True), weighted)
 
     def lanes_of(row):
         return jnp.where(low, to_column(row, TOTAL), to_column(row, TOTAL + SEQS))

time: 60 us -> 59.5 us (level)
  no operation moved by 1% of the time
where the time goes in v4:
time: 59.5 us; the launch traced here: 59.3 us
  blocking collectives  53.8 us (90%)
  Pallas kernels  4.24 us (7%)
  between operations  0.65 us (1%)
  other arithmetic  0.6 us (1%)
    all_to_all x2, blocking collectives, exchange(): lax.all_to_all(slots.reshape(N_KV, 1, ROWS * LANES), KV, 0, 0, tiled=True)  48.4 us
    all_gather x1, blocking collectives, on_device(): mixed = lax.all_gather(partial_out, 'tp').sum(0)  5.34 us
    pallas_call x3, Pallas kernels, call(): return run(*operands)  4.24 us

profile of v4, /device:TPU:1, one launch (start us, length us, event | category | flops | bytes accessed | tf_op | source)
XLA Modules:
  0.0 59.3 jit_solution(6266733923640989793)
XLA Ops:
  0.6 1.9 %prep.1 = (f32[576,128]{1,0:T(8,128)S(1)}, f32[16,512]{1,0:T(8,128)S(1)}, bf16[8,2,64,512]{3,2,1,0:T(8,128)(2,1)S(1)}, bf16[8,2,64,512]{3,2,1,0:T(8,128)(2,1)S(1)}, bf16[2,16,64]{2,1,0:T(8,128)(2,1)S(1)}) custom-call(bf16[8,16]{1,0:T(8,128)(2,1)} %refs_0_.1, f32[1,16]{1,0:T(1,128)} %bitcast.22, bf16[16,2,64]{2,1,0:T(2,128)(2,1)} %refs_2_.1, ...), custom_call_target="tpu_custom_call" | custom-call | tf_op jit(solution)/shard_map/prep/pallas_call | solution.py:263
  2.5 30.8 %all_to_all.10 = f32[64,1,1152]{2,1,0:T(1,128)S(1)} all-to-all(f32[64,1,1152]{2,1,0:T(1,128)S(1)} %bitcast.17), channel_id=1, replica_groups=mesh['dp'=4,'kv_0'=8,'kv_1'=8,'tp'=2] {'kv_0','kv_1'}, dimensions={0} | all-to-all | bytes 589824 | tf_op jit(solution)/shard_map/all_to_all | solution.py:255
  33.3 1.1 %attend.1 = (f32[576,128]{1,0:T(8,128)S(1)}, f32[8,128]{1,0:T(8,128)S(1)}, f32[8,128]{1,0:T(8,128)S(1)}, f32[64,128]{1,0:T(8,128)S(1)}, f32[2,8]{1,0:T(2,128)}) custom-call(f32[576,128]{1,0:T(8,128)S(1)} %bitcast.14, bf16[8,2,64,512]{3,2,1,0:T(8,128)(2,1)S(1)} %get-tuple-element.18.cache_key, bf16[8,2,64,512]{3,2,1,0:T(8,128)(2,1)S(1)} %get-tuple-element.19.cache_value, ...), custom_call_target="tpu_custom_call" | custom-call | tf_op jit(solution)/shard_map/attend/pallas_call | solution.py:263
  34.4 17.6 %all_to_all.11 = f32[64,1,1152]{2,1,0:T(1,128)S(1)} all-to-all(f32[64,1,1152]{2,1,0:T(1,128)S(1)} %bitcast.16), channel_id=1, replica_groups=mesh['dp'=4,'kv_0'=8,'kv_1'=8,'tp'=2] {'kv_0','kv_1'}, dimensions={0} | all-to-all | bytes 589824 | tf_op jit(solution)/shard_map/all_to_all | solution.py:255
  52.0 1.3 %combine.1 = (f32[8,16]{1,0:T(8,128)S(1)}, bf16[8,2,64]{2,1,0:T(2,128)(2,1)}, f32[8,2,64]{2,1,0:T(2,128)}) custom-call(f32[576,128]{1,0:T(8,128)S(1)} %bitcast.15, f32[8,128]{1,0:T(8,128)S(1)} %get-tuple-element.22.query, f32[8,128]{1,0:T(8,128)S(1)} %get-tuple-element.23.sums, f32[64,128]{1,0:T(8,128)S(1)} %get-tuple-element.24.shift, ...), custom_call_target="tpu_custom_call" | custom-call | tf_op jit(solution)/shard_map/combine/pallas_call | solution.py:263
  53.3 5.3 %all-gather = f32[16,16]{1,0:T(8,128)S(1)} all-gather(f32[8,16]{1,0:T(8,128)S(1)} %get-tuple-element.26), channel_id=2, replica_groups=mesh['dp'=4,'kv_0'=8,'kv_1'=8,'tp'=2] {'tp'}, dimensions={0}, use_global_device_ids=true | all-gather | bytes 1536 | tf_op jit(solution)/shard_map/all_gather | solution.py:308
  58.7 0.6 %bitcast_reduce_fusion = f32[8,16]{1,0:T(8,128)} fusion(f32[16,16]{1,0:T(8,128)S(1)} %all-gather), kind=kLoop, calls=%fused_computation | loop fusion | flops 128 | bytes 1536 | tf_op jit(solution)/shard_map/reduce_sum | solution.py:308

commit v5 on v4

--- a/solution.py
+++ b/solution.py
@@ -95,14 +95,11 @@
     squares = jnp.sum(wide * wide, axis=1, keepdims=True)
     scaled = wide * gain[...]
 
-    def project(weight):
-        weight = weight[...].astype(F32)
-        halves = [
-            jnp.dot(scaled, weight[:, h, :], precision=HI, preferred_element_type=F32)
-            for h in range(2)
-        ]
-        return jnp.concatenate(halves, axis=1)
-
+    wide_weights = [w[...].astype(F32) for w in (w_query, w_key, w_value, w_gate)]
+    halves = [w[:, h, :] for w in wide_weights for h in range(2)]
+    products = jnp.dot(
+        scaled, jnp.concatenate(halves, axis=1), precision=HI, preferred_element_type=F32
+    )
     forget = lax.dot_general(
         scaled, w_forget[...].astype(F32), NT, precision=HI, preferred_element_type=F32
     )
@@ -113,19 +110,24 @@
     shape = (LANES, LANES)
     upper = (iota(shape, 0) > iota(shape, 1)).astype(F32)
     row = to_row(squares, 0)
-    for h in range(2):
-        gates = jnp.where(live, logf[:, h, :], F32(0.0))
+    blocks = SPAN // LANES
+    gates = []
+    for h in range(2):
+        masked = jnp.where(live, logf[:, h, :], F32(0.0))
+        gates += [masked[:, LANES * b : LANES * (b + 1)] for b in range(blocks)]
+    inside = jnp.dot(
+        jnp.concatenate(gates, axis=0), upper, precision=HI, preferred_element_type=F32
+    )
+    for h in range(2):
         biases, after = [], jnp.zeros((SEQS, 1), F32)
-        for b in reversed(range(SPAN // LANES)):
-            part = gates[:, LANES * b : LANES * (b + 1)]
-            biases.append(jnp.dot(part, upper, precision=HI, preferred_element_type=F32) + after)
-            after = after + jnp.sum(part, axis=1, keepdims=True)
+        for n in reversed(range(blocks * h, blocks * (h + 1))):
+            biases.append(inside[SEQS * n : SEQS * (n + 1)] + after)
+            after = after + jnp.sum(gates[n], axis=1, keepdims=True)
         bias = jnp.concatenate(biases[::-1], axis=1)
         bias_out[pl.ds(SEQS * h, SEQS), :] = jnp.where(live, bias, F32(very_low))
         row = row + to_row(forget[:, h : h + 1], FORGET + SEQS * h)
         row = row + to_row(after, TOTAL + SEQS * h)
-    query = project(w_query)
-    parts = [project(w) for w in (w_key, w_value, w_gate)]
+    query, *parts = [products[:, LANES * n : LANES * (n + 1)] for n in range(4)]
     fill(slots, query)
     for c in range(8):
         tail = jnp.broadcast_to(row, (SEQS, LANES))
@@ -139,7 +141,7 @@
 
 
 def attend(
-    slots, cache_key, cache_value, bias, send, query_out, sums_out, shift_out, logf_out
+    slots, cache_key, cache_value, bias, send, query_out, sums_out, shift_out, logf_out, logf_here, sem
 ):
     seq = iota((SEQS, LANES), 0)
     raw = jnp.zeros((SEQS, LANES), F32)
@@ -155,8 +157,10 @@
     for h in range(2):
         forget = to_column(sums, FORGET + SEQS * h) * inv_root
         logf = jnp.minimum(forget, 0.0) - jnp.log1p(jnp.exp(-jnp.abs(forget)))
-        logf_out[pl.ds(h, 1), :] = to_row(logf, 0)[:, :SEQS]
+        logf_here[pl.ds(h, 1), :] = to_row(logf, 0)[:, :SEQS]
         logf_row = logf_row + to_row(logf, TOTAL + SEQS * h)
+    copy = pltpu.make_async_copy(logf_here, logf_out, sem)
+    copy.start()
     tails = slots[pl.ds(SEQS, N_KV, stride=ROWS), :]
     shape = (N_KV, N_KV)
     upper = (iota(shape, 1) > iota(shape, 0)).astype(F32)
@@ -196,9 +200,12 @@
     fill(send, local)
     for c in range(8):
         send[pl.ds(ROWS * c + SEQS, SEQS, stride=ROWS * 8), :] = tail
-
-
-def combine(slots, query, sums, shift, w_out, partial_out, key_out, value_out):
+    copy.wait()
+
+
+def combine(
+    slots, query, sums, shift, w_out, partial_out, key_out, value_out, key_here, value_here, sems
+):
     sums_row = sums[0:1, :]
     inv_root = lax.rsqrt(to_column(sums_row, 0) * (1.0 / D) + eps)
     parts = [jnp.zeros((SEQS, LANES), F32) for _ in range(3)]
@@ -212,8 +219,14 @@
     key = head_norm(key).astype(jnp.bfloat16)
     for h in range(2):
         part = slice(HEAD_DIM * h, HEAD_DIM * (h + 1))
-        key_out[:, h, :] = key[:, part]
-        value_out[:, h, :] = value[:, part]
+        key_here[:, h, :] = key[:, part]
+        value_here[:, h, :] = value[:, part]
+    copies = [
+        pltpu.make_async_copy(key_here, key_out, sems.at[0]),
+        pltpu.make_async_copy(value_here, value_out, sems.at[1]),
+    ]
+    for copy in copies:
+        copy.start()
     score_new = [x * HEAD_DIM ** (-0.5) for x in per_head(query[...] * key.astype(F32))]
     tails = slots[pl.ds(SEQS, N_KV, stride=ROWS), :]
     score_row = jnp.zeros((1, LANES), F32)
@@ -249,6 +262,8 @@
         half = gated[:, HEAD_DIM * h : HEAD_DIM * (h + 1)]
         mixed = mixed + lax.dot_general(half, w_out[h], NT, preferred_element_type=F32)
     partial_out[...] = mixed
+    for copy in copies:
+        copy.wait()
 
 
 def exchange(slots):
@@ -256,8 +271,13 @@
     return slots.reshape(N_KV * ROWS, LANES)
 
 
-def call(kernel, name, outs, operands, **more):
-    shapes = [jax.ShapeDtypeStruct(shape, dtype) for shape, dtype in outs]
+def call(kernel, name, outs, operands, leaving=0, **more):
+    kept = len(outs) - leaving
+    shapes = [jax.ShapeDtypeStruct(shape, dtype) for shape, dtype in outs[:kept]]
+    if leaving:
+        shapes += [pltpu.HBM(shape, dtype) for shape, dtype in outs[kept:]]
+        specs = [pltpu.VMEM] * kept + [pltpu.HBM] * leaving
+        more["out_specs"] = [pl.BlockSpec(memory_space=space) for space in specs]
     params = pltpu.CompilerParams(vmem_limit_bytes=VMEM)
     run = pl.pallas_call(kernel, out_shape=shapes, name=name, compiler_params=params, **more)
     return run(*operands)
@@ -297,6 +317,8 @@
         "attend",
         [whole, tile, tile, ((N_KV, LANES), F32), ((2, SEQS), F32)],
         (exchange(first), keys, values, bias),
+        leaving=1,
+        scratch_shapes=[pltpu.VMEM((2, SEQS), F32), pltpu.SemaphoreType.DMA],
     )
     heads = (SEQS, 2, HEAD_DIM)
     partial_out, key_new, value_new = call(
@@ -304,6 +326,12 @@
         "combine",
         [((SEQS, tokens.shape[1]), F32), (heads, jnp.bfloat16), (heads, F32)],
         (exchange(second), query, sums, shift, w_out),
+        leaving=2,
+        scratch_shapes=[
+            pltpu.VMEM(heads, jnp.bfloat16),
+            pltpu.VMEM(heads, F32),
+            pltpu.SemaphoreType.DMA((2,)),
+        ],
     )
     mixed = lax.all_gather(partial_out, "tp").sum(0)
     return mixed, key_new, value_new, jnp.transpose(logf_new)

time: 59.5 us -> 59.4 us (level)
  no operation moved by 1% of the time
where the time goes in v5:
time: 59.4 us; the launch traced here: 59.2 us
  blocking collectives  53.8 us (91%)
  Pallas kernels  4.1 us (7%)
  between operations  0.66 us (1%)
  other arithmetic  0.6 us (1%)
    all_to_all x2, blocking collectives, exchange(): lax.all_to_all(slots.reshape(N_KV, 1, ROWS * LANES), KV, 0, 0, tiled=True)  48.4 us
    all_gather x1, blocking collectives, on_device(): mixed = lax.all_gather(partial_out, 'tp').sum(0)  5.35 us
    pallas_call x3, Pallas kernels, call(): return run(*operands)  4.1 us

profile of v5, /device:TPU:1, one launch (start us, length us, event | category | flops | bytes accessed | tf_op | source)
XLA Modules:
  0.0 59.2 jit_solution(8016637792530175483)
XLA Ops:
  0.6 1.8 %prep.1 = (f32[576,128]{1,0:T(8,128)S(1)}, f32[16,512]{1,0:T(8,128)S(1)}, bf16[8,2,64,512]{3,2,1,0:T(8,128)(2,1)S(1)}, bf16[8,2,64,512]{3,2,1,0:T(8,128)(2,1)S(1)}, bf16[2,16,64]{2,1,0:T(8,128)(2,1)S(1)}) custom-call(bf16[8,16]{1,0:T(8,128)(2,1)} %refs_0_.1, f32[1,16]{1,0:T(1,128)} %bitcast.22, bf16[16,2,64]{2,1,0:T(2,128)(2,1)} %refs_2_.1, ...), custom_call_target="tpu_custom_call" | custom-call | tf_op jit(solution)/shard_map/prep/pallas_call | solution.py:283
  2.4 30.8 %all_to_all.10 = f32[64,1,1152]{2,1,0:T(1,128)S(1)} all-to-all(f32[64,1,1152]{2,1,0:T(1,128)S(1)} %bitcast.17), channel_id=1, replica_groups=mesh['dp'=4,'kv_0'=8,'kv_1'=8,'tp'=2] {'kv_0','kv_1'}, dimensions={0} | all-to-all | bytes 589824 | tf_op jit(solution)/shard_map/all_to_all | solution.py:270
  33.2 1.1 %attend.1 = (f32[576,128]{1,0:T(8,128)S(1)}, f32[8,128]{1,0:T(8,128)S(1)}, f32[8,128]{1,0:T(8,128)S(1)}, f32[64,128]{1,0:T(8,128)S(1)}, f32[2,8]{1,0:T(2,128)}) custom-call(f32[576,128]{1,0:T(8,128)S(1)} %bitcast.14, bf16[8,2,64,512]{3,2,1,0:T(8,128)(2,1)S(1)} %get-tuple-element.18.cache_key, bf16[8,2,64,512]{3,2,1,0:T(8,128)(2,1)S(1)} %get-tuple-element.19.cache_value, ...), custom_call_target="tpu_custom_call" | custom-call | tf_op jit(solution)/shard_map/attend/pallas_call | solution.py:283
  34.4 17.6 %all_to_all.11 = f32[64,1,1152]{2,1,0:T(1,128)S(1)} all-to-all(f32[64,1,1152]{2,1,0:T(1,128)S(1)} %bitcast.16), channel_id=1, replica_groups=mesh['dp'=4,'kv_0'=8,'kv_1'=8,'tp'=2] {'kv_0','kv_1'}, dimensions={0} | all-to-all | bytes 589824 | tf_op jit(solution)/shard_map/all_to_all | solution.py:270
  52.0 1.2 %combine.1 = (f32[8,16]{1,0:T(8,128)S(1)}, bf16[8,2,64]{2,1,0:T(2,128)(2,1)}, f32[8,2,64]{2,1,0:T(2,128)}) custom-call(f32[576,128]{1,0:T(8,128)S(1)} %bitcast.15, f32[8,128]{1,0:T(8,128)S(1)} %get-tuple-element.22.query, f32[8,128]{1,0:T(8,128)S(1)} %get-tuple-element.23.sums, f32[64,128]{1,0:T(8,128)S(1)} %get-tuple-element.24.shift, ...), custom_call_target="tpu_custom_call" | custom-call | tf_op jit(solution)/shard_map/combine/pallas_call | solution.py:283
  53.2 5.4 %all-gather = f32[16,16]{1,0:T(8,128)S(1)} all-gather(f32[8,16]{1,0:T(8,128)S(1)} %get-tuple-element.26), channel_id=2, replica_groups=mesh['dp'=4,'kv_0'=8,'kv_1'=8,'tp'=2] {'tp'}, dimensions={0}, use_global_device_ids=true | all-gather | bytes 1536 | tf_op jit(solution)/shard_map/all_gather | solution.py:336
  58.6 0.6 %bitcast_reduce_fusion = f32[8,16]{1,0:T(8,128)} fusion(f32[16,16]{1,0:T(8,128)S(1)} %all-gather), kind=kLoop, calls=%fused_computation | loop fusion | flops 128 | bytes 1536 | tf_op jit(solution)/shard_map/reduce_sum | solution.py:336

commit v6 on v5

--- a/solution.py
+++ b/solution.py
@@ -86,7 +86,7 @@
         pltpu.make_async_copy(source, target, sems.at[n])
         for n, (source, target) in enumerate(zip(sources, targets))
     ]
-    for copy in copies:
+    for copy in copies[:9] + copies[11:] + copies[9:11]:
         copy.start()
     for copy in copies[:9]:
         copy.wait()

time: 59.4 us -> 59.4 us (level)
  no operation moved by 1% of the time
where the time goes in v6:
time: 59.4 us; the launch traced here: 59.2 us
  blocking collectives  53.8 us (91%)
  Pallas kernels  4.1 us (7%)
  between operations  0.66 us (1%)
  other arithmetic  0.6 us (1%)
    all_to_all x2, blocking collectives, exchange(): lax.all_to_all(slots.reshape(N_KV, 1, ROWS * LANES), KV, 0, 0, tiled=True)  48.4 us
    all_gather x1, blocking collectives, on_device(): mixed = lax.all_gather(partial_out, 'tp').sum(0)  5.35 us
    pallas_call x3, Pallas kernels, call(): return run(*operands)  4.1 us

profile of v6, /device:TPU:1, one launch (start us, length us, event | category | flops | bytes accessed | tf_op | source)
XLA Modules:
  0.0 59.2 jit_solution(7226321480555241717)
XLA Ops:
  0.6 1.8 %prep.1 = (f32[576,128]{1,0:T(8,128)S(1)}, f32[16,512]{1,0:T(8,128)S(1)}, bf16[8,2,64,512]{3,2,1,0:T(8,128)(2,1)S(1)}, bf16[8,2,64,512]{3,2,1,0:T(8,128)(2,1)S(1)}, bf16[2,16,64]{2,1,0:T(8,128)(2,1)S(1)}) custom-call(bf16[8,16]{1,0:T(8,128)(2,1)} %refs_0_.1, f32[1,16]{1,0:T(1,128)} %bitcast.22, bf16[16,2,64]{2,1,0:T(2,128)(2,1)} %refs_2_.1, ...), custom_call_target="tpu_custom_call" | custom-call | tf_op jit(solution)/shard_map/prep/pallas_call | solution.py:283
  2.4 30.8 %all_to_all.10 = f32[64,1,1152]{2,1,0:T(1,128)S(1)} all-to-all(f32[64,1,1152]{2,1,0:T(1,128)S(1)} %bitcast.17), channel_id=1, replica_groups=mesh['dp'=4,'kv_0'=8,'kv_1'=8,'tp'=2] {'kv_0','kv_1'}, dimensions={0} | all-to-all | bytes 589824 | tf_op jit(solution)/shard_map/all_to_all | solution.py:270
  33.2 1.1 %attend.1 = (f32[576,128]{1,0:T(8,128)S(1)}, f32[8,128]{1,0:T(8,128)S(1)}, f32[8,128]{1,0:T(8,128)S(1)}, f32[64,128]{1,0:T(8,128)S(1)}, f32[2,8]{1,0:T(2,128)}) custom-call(f32[576,128]{1,0:T(8,128)S(1)} %bitcast.14, bf16[8,2,64,512]{3,2,1,0:T(8,128)(2,1)S(1)} %get-tuple-element.18.cache_key, bf16[8,2,64,512]{3,2,1,0:T(8,128)(2,1)S(1)} %get-tuple-element.19.cache_value, ...), custom_call_target="tpu_custom_call" | custom-call | tf_op jit(solution)/shard_map/attend/pallas_call | solution.py:283
  34.4 17.6 %all_to_all.11 = f32[64,1,1152]{2,1,0:T(1,128)S(1)} all-to-all(f32[64,1,1152]{2,1,0:T(1,128)S(1)} %bitcast.16), channel_id=1, replica_groups=mesh['dp'=4,'kv_0'=8,'kv_1'=8,'tp'=2] {'kv_0','kv_1'}, dimensions={0} | all-to-all | bytes 589824 | tf_op jit(solution)/shard_map/all_to_all | solution.py:270
  52.0 1.2 %combine.1 = (f32[8,16]{1,0:T(8,128)S(1)}, bf16[8,2,64]{2,1,0:T(2,128)(2,1)}, f32[8,2,64]{2,1,0:T(2,128)}) custom-call(f32[576,128]{1,0:T(8,128)S(1)} %bitcast.15, f32[8,128]{1,0:T(8,128)S(1)} %get-tuple-element.22.query, f32[8,128]{1,0:T(8,128)S(1)} %get-tuple-element.23.sums, f32[64,128]{1,0:T(8,128)S(1)} %get-tuple-element.24.shift, ...), custom_call_target="tpu_custom_call" | custom-call | tf_op jit(solution)/shard_map/combine/pallas_call | solution.py:283
  53.2 5.4 %all-gather = f32[16,16]{1,0:T(8,128)S(1)} all-gather(f32[8,16]{1,0:T(8,128)S(1)} %get-tuple-element.26), channel_id=2, replica_groups=mesh['dp'=4,'kv_0'=8,'kv_1'=8,'tp'=2] {'tp'}, dimensions={0}, use_global_device_ids=true | all-gather | bytes 1536 | tf_op jit(solution)/shard_map/all_gather | solution.py:336
  58.6 0.6 %bitcast_reduce_fusion = f32[8,16]{1,0:T(8,128)} fusion(f32[16,16]{1,0:T(8,128)S(1)} %all-gather), kind=kLoop, calls=%fused_computation | loop fusion | flops 128 | bytes 1536 | tf_op jit(solution)/shard_map/reduce_sum | solution.py:336
